TPU v7x, 32 devices: a whole 2x2x4 slice. The times are simulated.
32 devices in a mesh: sp: 16 (over z, y, x), tp: 2 (over core).
Axes of the slice: x: 2, y: 2, z: 4, core: 2. Of those that a mesh axis runs over, the one named last changes fastest.
Arguments:
- inputs: bfloat16 [6144, 2048], P(('sp', 'tp')), may hold values from -6 to 6
- norm_gain: float32 [2048], replicated, may hold values from 0.1 to 1.9
- latent_down: bfloat16 [2048, 256], P('sp'), may hold values from -0.125 to 0.125
- rope_down: bfloat16 [2048, 64], P('sp'), may hold values from -0.125 to 0.125
- latent_gain: float32 [256], replicated, may hold values from 0.1 to 1.9
- mla_query: bfloat16 [2048, 1536], P(None, 'tp'), as said below
- key_up: bfloat16 [256, 1024], replicated, may hold values from -3.5 to 3.5
- value_up: bfloat16 [256, 1024], replicated, may hold values from -1.75 to 1.75
- swa_query: bfloat16 [2048, 1024], P(None, 'tp'), as said below
- swa_key: bfloat16 [2048, 512], P(None, 'tp'), may hold values from -0.125 to 0.125
- swa_value: bfloat16 [2048, 512], P(None, 'tp'), may hold values from -0.125 to 0.125
- sink_logits: float32 [16], replicated, may hold values from 1 to 6
- out_mla: bfloat16 [1024, 2048], P(None, 'tp'), may hold values from -0.875 to 0.875
- out_swa: bfloat16 [1024, 2048], P(None, 'tp'), may hold values from -0.875 to 0.875
Outputs:
- mixed: bfloat16 [6144, 2048], P('sp', 'tp')
Inputs may be any that keep to these rules, and one draw needn't show every extreme that they name: `mla_query`: entries lie within 360 / sqrt(2048) in magnitude. `swa_query`: entries lie within 900 / sqrt(2048) in magnitude.
All inputs are finite; a program needn't handle non-finite values.
Results may differ from a plain program's by a relative error of at most 0.02.
The roundings to bfloat16 on the way count: a program that leaves them out, or rounds other values in their place, can miss the bound.
Values may be sent and summed in bfloat16 or wider, within the bound.
A program may use at most 64 MiB of HBM per device.

v0:
```python
import math

import jax
import jax.numpy as jnp
from jax import lax
from jax.experimental import pallas as pl
from jax.experimental.pallas import tpu as pltpu
from jax.sharding import PartitionSpec as P

NOPE = 128
ROPE = 64
VDIM = 128
KV_RANK = 256
HEAD = 64
WINDOW = 128


NORM_EPS = 1e-06
ROPE_BASE = 10000.0
MASKED_VALUE = -1e30
KEY_SPAN = 512


def from_behind(value, axis, steps):
    count = lax.axis_size(axis)
    first, last = (max(0, -steps), min(count, count - steps))
    return lax.ppermute(value, axis, [(source, source + steps) for source in range(first, last)])


def to_float(values):
    return lax.optimization_barrier(values).astype(jnp.float32)


def norm_rows(values, gains):
    widened = to_float(values)
    scaled = widened * lax.rsqrt(jnp.mean(widened * widened, axis=-1, keepdims=True) + NORM_EPS)
    return (scaled * gains).astype(jnp.bfloat16)


def rotate(values, positions):
    full_width = values.shape[-1]
    half_width = full_width // 2
    inverse = ROPE_BASE ** (-jnp.arange(0, full_width, 2, dtype=jnp.float32) / full_width)
    angles = positions.astype(jnp.float32)[:, None] * inverse[None, :]
    shaped = (values.shape[0],) + (1,) * (values.ndim - 2) + (half_width,)
    cos_table = jnp.cos(angles).reshape(shaped)
    sin_table = jnp.sin(angles).reshape(shaped)
    widened = to_float(values)
    first_half = widened[..., :half_width]
    second_half = widened[..., half_width:]
    return jnp.concatenate(
        [
            first_half * cos_table - second_half * sin_table,
            first_half * sin_table + second_half * cos_table,
        ],
        axis=-1,
    ).astype(jnp.bfloat16)


def attend_latent(
    state_in, keys_latent, keys_rope, key_positions, query_latent, query_rope, query_pos, mla_scale
):
    key_count = keys_latent.shape[0]
    span_rows = math.gcd(key_count, KEY_SPAN)
    last_query = query_pos[-1]

    def update(step_index, state):
        span_pos = lax.dynamic_slice_in_dim(key_positions, step_index * span_rows, span_rows, 0)

        def compute(current):
            running_max, denom_sum, weighted = current
            lat_block = lax.dynamic_slice_in_dim(keys_latent, step_index * span_rows, span_rows, 0)
            rope_block = lax.dynamic_slice_in_dim(keys_rope, step_index * span_rows, span_rows, 0)
            scores = (
                jnp.einsum(
                    "htj,sj->hts", query_latent, lat_block, preferred_element_type=jnp.float32
                )
                + jnp.einsum(
                    "htd,sd->hts", query_rope, rope_block, preferred_element_type=jnp.float32
                )
            ) * mla_scale
            allowed = span_pos[None, None, :] <= query_pos[None, :, None]
            scores = jnp.where(allowed, scores, MASKED_VALUE)
            new_max = jnp.maximum(running_max, jnp.max(scores, axis=-1))
            weights_raw = jnp.where(allowed, jnp.exp(scores - new_max[..., None]), 0.0)
            rescale = jnp.exp(running_max - new_max)
            denom_sum = denom_sum * rescale + jnp.sum(weights_raw, axis=-1)
            weighted = weighted * rescale[..., None] + jnp.einsum(
                "hts,sj->htj",
                weights_raw.astype(jnp.bfloat16),
                lat_block,
                preferred_element_type=jnp.float32,
            )
            return (new_max, denom_sum, weighted)

        return lax.cond(span_pos[0] <= last_query, compute, lambda current: current, state)

    return lax.fori_loop(0, key_count // span_rows, update, state_in)


def shards(
    inputs,
    norm_gain,
    latent_down,
    rope_down,
    latent_gain,
    mla_query,
    key_up,
    value_up,
    swa_query,
    swa_key,
    swa_value,
    sink_logits,
    out_mla,
    out_swa,
):
    own_rows = inputs.shape[0]
    tp_count = lax.axis_size("tp")
    block_rows = own_rows * tp_count
    tp_rank = lax.axis_index("tp")
    offset = lax.axis_index("sp") * block_rows
    own_pos = offset + tp_rank * own_rows + jnp.arange(own_rows, dtype=jnp.int32)
    block_pos = offset + jnp.arange(block_rows, dtype=jnp.int32)
    width_mla = mla_query.shape[1]
    width_swa = swa_query.shape[1]
    width_kv = swa_key.shape[1]
    heads_mla = width_mla // (NOPE + ROPE)
    heads_swa = width_swa // HEAD
    groups_kv = width_kv // HEAD
    group = heads_swa // groups_kv
    normed = norm_rows(inputs, norm_gain)
    pieces = lax.all_gather(normed, "tp", axis=0, tiled=True)
    projected = jnp.concatenate(
        [
            jnp.dot(pieces, mla_query, preferred_element_type=jnp.float32).astype(jnp.bfloat16),
            jnp.dot(pieces, swa_query, preferred_element_type=jnp.float32).astype(jnp.bfloat16),
            jnp.dot(pieces, swa_key, preferred_element_type=jnp.float32).astype(jnp.bfloat16),
            jnp.dot(pieces, swa_value, preferred_element_type=jnp.float32).astype(jnp.bfloat16),
        ],
        axis=1,
    )
    pieces = (
        lax.all_gather(latent_down, "sp", axis=0, tiled=True),
        lax.all_gather(rope_down, "sp", axis=0, tiled=True),
    )
    latent = jnp.dot(normed, pieces[0], preferred_element_type=jnp.float32)
    rope_raw = jnp.dot(normed, pieces[1], preferred_element_type=jnp.float32)
    keys_latent = norm_rows(latent.astype(jnp.bfloat16), latent_gain)
    keys_rope = rotate(rope_raw.astype(jnp.bfloat16), own_pos)
    queries = projected[:, :width_mla].reshape(block_rows, heads_mla, NOPE + ROPE)
    query_rope = jnp.transpose(rotate(queries[:, :, NOPE:], block_pos), (1, 0, 2))
    head_first = tp_rank * heads_mla
    up_keys = lax.dynamic_slice_in_dim(key_up, head_first * NOPE, heads_mla * NOPE, 1)
    up_keys = up_keys.reshape(KV_RANK, heads_mla, NOPE)
    query_latent = jnp.einsum(
        "thn,jhn->htj", queries[:, :, :NOPE], up_keys, preferred_element_type=jnp.float32
    ).astype(jnp.bfloat16)
    mla_scale = (NOPE + ROPE) ** (-0.5)
    every_latent, every_rope = (
        lax.all_gather(query_latent, "tp", axis=0, tiled=True),
        lax.all_gather(query_rope, "tp", axis=0, tiled=True),
    )
    slice_latent, slice_rope = (
        lax.all_gather(keys_latent, "sp", axis=0, tiled=True),
        lax.all_gather(keys_rope, "sp", axis=0, tiled=True),
    )
    heads_all = every_latent.shape[0]
    row_index = jnp.arange(slice_latent.shape[0], dtype=jnp.int32)
    slice_pos = row_index // own_rows * block_rows + tp_rank * own_rows + row_index % own_rows
    slice_state = (
        jnp.full((heads_all, block_rows), MASKED_VALUE, jnp.float32),
        jnp.zeros((heads_all, block_rows), jnp.float32),
        jnp.zeros((heads_all, block_rows, KV_RANK), jnp.float32),
    )
    part_max, part_sum, part_weighted = attend_latent(
        slice_state,
        slice_latent,
        slice_rope,
        slice_pos,
        every_latent,
        every_rope,
        block_pos,
        mla_scale,
    )
    global_max = lax.pmax(part_max, "tp")
    rescale = jnp.exp(part_max - global_max)
    denom_sum, weighted = (
        lax.psum_scatter(
            (part_sum * rescale).astype(jnp.bfloat16), "tp", scatter_dimension=0, tiled=True
        ).astype(jnp.float32),
        lax.psum_scatter(
            (part_weighted * rescale[..., None]).astype(jnp.bfloat16),
            "tp",
            scatter_dimension=0,
            tiled=True,
        ).astype(jnp.float32),
    )
    latent_out = (weighted / denom_sum[..., None]).astype(jnp.bfloat16)
    up_values = lax.dynamic_slice_in_dim(value_up, head_first * VDIM, heads_mla * VDIM, 1)
    up_values = up_values.reshape(KV_RANK, heads_mla, VDIM)
    mla_out = jnp.einsum(
        "htj,jhv->thv", latent_out, up_values, preferred_element_type=jnp.float32
    ).astype(jnp.bfloat16)
    mla_out = mla_out.reshape(block_rows, heads_mla * VDIM)
    swa_q = projected[:, width_mla : width_mla + width_swa].reshape(
        block_rows, groups_kv, group, HEAD
    )
    swa_k = projected[:, width_mla + width_swa : width_mla + width_swa + width_kv]
    swa_v = projected[:, width_mla + width_swa + width_kv : width_mla + width_swa + 2 * width_kv]
    prev_keys, prev_values = from_behind(
        (swa_k[block_rows - WINDOW :], swa_v[block_rows - WINDOW :]), "sp", 1
    )
    window_keys_all = jnp.concatenate([prev_keys, swa_k], axis=0).reshape(
        WINDOW + block_rows, groups_kv, HEAD
    )
    window_values = jnp.concatenate([prev_values, swa_v], axis=0).reshape(
        WINDOW + block_rows, groups_kv, HEAD
    )
    scores = jnp.einsum(
        "tkgd,skd->kgts", swa_q, window_keys_all, preferred_element_type=jnp.float32
    ) * HEAD ** (-0.5)
    key_pos = offset - WINDOW + jnp.arange(WINDOW + block_rows, dtype=jnp.int32)
    distance = block_pos[:, None] - key_pos[None, :]
    allowed = (distance >= 0) & (distance < WINDOW) & (key_pos[None, :] >= 0)
    scores = jnp.where(allowed, scores, MASKED_VALUE)
    sink_table = lax.dynamic_slice_in_dim(sink_logits, tp_rank * heads_swa, heads_swa, 0)
    sink_table = sink_table.reshape(groups_kv, group, 1, 1)
    row_max = jnp.maximum(jnp.max(scores, axis=-1, keepdims=True), sink_table)
    weights_raw = jnp.exp(scores - row_max)
    weights = (
        weights_raw / (jnp.sum(weights_raw, axis=-1, keepdims=True) + jnp.exp(sink_table - row_max))
    ).astype(jnp.bfloat16)
    swa_out = jnp.einsum(
        "kgts,skd->tkgd", weights, window_values, preferred_element_type=jnp.float32
    ).astype(jnp.bfloat16)
    swa_out = swa_out.reshape(block_rows, heads_swa * HEAD)
    all_mla, all_swa = (
        lax.all_gather(mla_out, "tp", axis=1, tiled=True),
        lax.all_gather(swa_out, "tp", axis=1, tiled=True),
    )
    mixed = jnp.dot(all_mla, out_mla, preferred_element_type=jnp.float32) + jnp.dot(
        all_swa, out_swa, preferred_element_type=jnp.float32
    )
    return mixed.astype(jnp.bfloat16)

MESH = pl.DeviceIdType.MESH
LOG2E = 1.4426950408889634
COPIES = 12
PLANE = 4


def normalize(values, gains):
    widened = values.astype(jnp.float32)
    scaled = widened * lax.rsqrt(jnp.mean(widened * widened, axis=-1, keepdims=True) + NORM_EPS)
    return (scaled * gains).astype(jnp.bfloat16)


def turn(values, cos, sin):
    half = values.shape[1] // 2
    widened = values.astype(jnp.float32)
    first, second = widened[:, :half], widened[:, half:]
    return jnp.concatenate(
        [first * cos - second * sin, first * sin + second * cos], axis=1
    ).astype(jnp.bfloat16)


def pack_rope(rope):
    rows = rope.shape[0] // 4
    return jnp.concatenate([rope[g * rows : (g + 1) * rows] for g in range(4)], axis=1)


def dot_f32(a, b):
    return jnp.dot(a, b, preferred_element_type=jnp.float32)


def dot_nt(a, b):
    return lax.dot_general(a, b, (((1,), (1,)), ((), ())), preferred_element_type=jnp.float32)


class Gather:
    def __init__(self, buf, send, recv, me, core, count):
        self.buf, self.send, self.recv, self.core = buf, send, recv, core
        self.me = me
        self.x = me + 1 - 2 * lax.rem(me, 2)
        self.y = me + 2 - 4 * lax.rem(lax.div(me, 2), 2)
        self.plane = lax.div(me, PLANE) * PLANE
        self.right = lax.rem(me + PLANE, count)
        self.left = lax.rem(me + count - PLANE, count)
        self.right_plane = lax.div(self.right, PLANE) * PLANE
        self.left_plane = lax.div(self.left, PLANE) * PLANE
        self.far = lax.rem(self.plane + 2 * PLANE, count)
        self.started = []

    def go(self, index, first, size, device):
        part = self.buf.at[pl.ds(first, size), pl.ds(self.core, 1)]
        copy = pltpu.make_async_remote_copy(
            src_ref=part,
            dst_ref=part,
            send_sem=self.send.at[index],
            recv_sem=self.recv.at[index],
            device_id=device,
            device_id_type=MESH,
        )
        copy.start()
        self.started.append(copy)
        return copy

    def pair(self, index, first, size):
        return self.go(index, first, size, {"tp": 1 - self.core})

    def step0(self):
        self.cx = self.go(0, self.me, 1, {"sp": self.x})
        self.p = [self.pair(6, self.me, 1)]

    def step1(self):
        self.cx.wait_recv()
        self.cy = self.go(1, lax.div(self.me, 2) * 2, 2, {"sp": self.y})
        self.p.append(self.pair(7, self.x, 1))

    def step2(self):
        self.cy.wait_recv()
        self.cr = self.go(2, self.plane, PLANE, {"sp": self.right})
        self.cl = self.go(3, self.plane, PLANE, {"sp": self.left})
        self.p.append(self.pair(8, lax.div(self.y, 2) * 2, 2))

    def step3(self):
        half = PLANE // 2
        self.cr.wait_recv()
        self.rr = self.go(4, self.left_plane, half, {"sp": self.right})
        self.p.append(self.pair(9, self.left_plane, PLANE))
        self.cl.wait_recv()
        self.rl = self.go(5, self.right_plane + half, half, {"sp": self.left})
        self.p.append(self.pair(10, self.right_plane, PLANE))

    def step4(self):
        self.rr.wait_recv()
        self.rl.wait_recv()
        self.p.append(self.pair(11, self.far, PLANE))

    def partner(self, first, last):
        for copy in self.p[first:last]:
            copy.wait_recv()

    def finish(self):
        for copy in self.started:
            copy.wait_send()


def layer_kernel(
    count,
    x_ref,
    gain_ref,
    down_ref,
    rope_down_ref,
    latent_gain_ref,
    cos_ref,
    sin_ref,
    key_up_ref,
    sink_ref,
    wq_ref,
    wsq_ref,
    wsk_ref,
    wsv_ref,
    value_up_ref,
    out_mla_ref,
    out_swa_ref,
    out_ref,
    keys_ref,
    queries,
    key_cat,
    key_t,
    top,
    total,
    acc,
    mla_all,
    swa_all,
    out_weights,
    weights,
    normed,
    proj,
    gathered,
    window,
    local_sem,
    wsend,
    wrecv,
    ksend,
    krecv,
    xsend,
    xrecv,
):
    me = lax.axis_index("sp")
    core = lax.axis_index("tp")
    own = x_ref.shape[0]
    block = 2 * own
    width_mla = wq_ref.shape[1]
    width_swa = wsq_ref.shape[1]
    width_kv = wsk_ref.shape[1]
    heads_mla = width_mla // (NOPE + ROPE)
    heads_swa = width_swa // HEAD
    group = width_swa // width_kv
    half_down = down_ref.shape[0] // 2

    loads, start = [], 0
    for i, ref in enumerate((wq_ref, wsq_ref, wsk_ref, wsv_ref)):
        width = ref.shape[1]
        loads.append(
            pltpu.make_async_copy(ref, weights.at[:, pl.ds(start, width)], local_sem.at[i])
        )
        loads[-1].start()
        start += width
    out_rows = out_mla_ref.shape[0]
    out_loads = []
    for i, ref in enumerate((out_mla_ref, out_swa_ref)):
        out_loads.append(
            pltpu.make_async_copy(
                ref, out_weights.at[pl.ds(i * out_rows, out_rows)], local_sem.at[4 + i]
            )
        )

    rows = pl.ds(pl.multiple_of(core * half_down, half_down), half_down)
    gathered[me, core, :half_down, :] = down_ref[rows, :]
    gathered[me, core, half_down:, :] = pack_rope(rope_down_ref[rows, :])

    wg = Gather(gathered, wsend, wrecv, me, core, count)
    kg = Gather(keys_ref, ksend, krecv, me, core, count)
    after = lax.rem(me + 1, count)
    before = lax.rem(me + count - 1, count)
    barrier = pltpu.get_barrier_semaphore()
    devices = [{"sp": d} for d in (wg.x, wg.y, wg.right, wg.left, after, before)]
    devices.append({"tp": 1 - core})
    for device in devices:
        pl.semaphore_signal(barrier, inc=1, device_id=device, device_id_type=MESH)
    pl.semaphore_wait(barrier, len(devices))
    wg.step0()

    mine = pl.multiple_of(core * own, own)
    other = pl.multiple_of((1 - core) * own, own)
    chunk = 32

    @pl.loop(0, own // chunk)
    def _(i):
        at = pl.multiple_of(i * chunk, chunk)
        normed[pl.ds(mine + at, chunk), :] = normalize(x_ref[pl.ds(at, chunk), :], gain_ref[...])

    part = normed.at[pl.ds(mine, own)]
    swap = pltpu.make_async_remote_copy(
        src_ref=part,
        dst_ref=part,
        send_sem=xsend.at[0],
        recv_sem=xrecv.at[0],
        device_id={"tp": 1 - core},
        device_id_type=MESH,
    )
    swap.start()
    wg.step1()
    for load in loads:
        load.wait()

    for load in out_loads:
        load.start()

    def project(at):
        lhs = normed[pl.ds(at, own), :]
        for j in range(0, proj.shape[1], 256):
            proj[pl.ds(at, own), j : j + 256] = dot_f32(lhs, weights[:, j : j + 256]).astype(
                jnp.bfloat16
            )

    wg.step2()
    project(mine)
    wg.step3()
    swap.wait_recv()
    project(other)
    wg.step4()

    kv = width_mla + width_swa
    window[WINDOW:, :] = proj[:, kv:]
    edge = pltpu.make_async_remote_copy(
        src_ref=window.at[pl.ds(block, WINDOW)],
        dst_ref=window.at[pl.ds(0, WINDOW)],
        send_sem=xsend.at[1],
        recv_sem=xrecv.at[1],
        device_id={"sp": after},
        device_id_type=MESH,
    )
    edge.start()
    queries[...] = jnp.zeros_like(queries)
    key_cat[...] = jnp.zeros_like(key_cat)
    cos, sin = cos_ref[...], sin_ref[...]
    for h in range(heads_mla):
        base = h * (NOPE + ROPE)
        up = key_up_ref[:, pl.ds(pl.multiple_of((core * heads_mla + h) * NOPE, NOPE), NOPE)]
        queries[h, :, :KV_RANK] = dot_nt(proj[:, base : base + NOPE], up).astype(jnp.bfloat16)
        queries[h, :, KV_RANK : KV_RANK + ROPE] = turn(proj[:, base + NOPE : base + NOPE + ROPE], cos, sin)
    wg.partner(0, 6)
    wg.finish()

    lhs = normed[pl.ds(mine, own), :]
    depth = lhs.shape[1]
    down = gathered[:, :, :half_down, :].reshape(depth, KV_RANK)
    packed = gathered[:, :, half_down:, :]
    rope_down = jnp.concatenate(
        [packed[:, :, :, g * ROPE : (g + 1) * ROPE] for g in range(4)], axis=2
    ).reshape(depth, ROPE)
    latent = dot_f32(lhs, down).astype(jnp.bfloat16)
    rope_raw = dot_f32(lhs, rope_down).astype(jnp.bfloat16)
    keys_ref[me, core, :own, :] = normalize(latent, latent_gain_ref[...])
    keys_rope = turn(rope_raw, cos_ref[pl.ds(mine, own), :], sin_ref[pl.ds(mine, own), :])
    keys_ref[me, core, own:, :] = pack_rope(keys_rope)
    kg.step0()

    row = lax.broadcasted_iota(jnp.int32, (WINDOW, 2 * WINDOW), 0)
    column = lax.broadcasted_iota(jnp.int32, (WINDOW, 2 * WINDOW), 1)
    distance = row + WINDOW - column
    inside = (distance >= 0) & (distance < WINDOW)

    def windowed(tile):
        allowed = inside
        if tile == 0:
            allowed = inside & ((column >= WINDOW) | (me > 0))
        at = tile * WINDOW
        outs = []
        for h in range(heads_swa):
            g = h // group
            q = proj[at : at + WINDOW, width_mla + h * HEAD : width_mla + (h + 1) * HEAD]
            k = window[at : at + 2 * WINDOW, g * HEAD : (g + 1) * HEAD]
            v = window[at : at + 2 * WINDOW, width_kv + g * HEAD : width_kv + (g + 1) * HEAD]
            scores = jnp.where(allowed, dot_nt(q, k) * HEAD ** (-0.5), MASKED_VALUE)
            sink = jnp.zeros((WINDOW, 1), jnp.float32) + sink_ref[core * heads_swa + h]
            top = jnp.maximum(jnp.max(scores, axis=-1, keepdims=True), sink)
            raw = jnp.exp(scores - top)
            total = jnp.sum(raw, axis=-1, keepdims=True) + jnp.exp(sink - top)
            outs.append(dot_f32((raw / total).astype(jnp.bfloat16), v).astype(jnp.bfloat16))
        swa_all[core, at : at + WINDOW, :] = jnp.concatenate(outs, axis=1)

    def swap_all(buf, index):
        part = buf.at[pl.ds(core, 1)]
        copy = pltpu.make_async_remote_copy(
            src_ref=part,
            dst_ref=part,
            send_sem=xsend.at[index],
            recv_sem=xrecv.at[index],
            device_id={"tp": 1 - core},
            device_id_type=MESH,
        )
        copy.start()
        return copy

    for tile in range(1, 2):
        windowed(tile)
    kg.step1()
    for tile in range(2, block // WINDOW):
        windowed(tile)
    edge.wait_recv()
    windowed(0)
    kg.step2()
    swa_swap = swap_all(swa_all, 2)

    top[...] = jnp.full_like(top, MASKED_VALUE)
    total[...] = jnp.zeros_like(total)
    acc[...] = jnp.zeros_like(acc)
    scale = (NOPE + ROPE) ** (-0.5) * LOG2E

    def update(j, diagonal):
        lat = keys_ref[j, :, :own, :].reshape(block, KV_RANK)
        packed = keys_ref[j, :, own:, :]
        rope = jnp.concatenate(
            [packed[:, :, g * ROPE : (g + 1) * ROPE] for g in range(4)], axis=1
        ).reshape(block, ROPE)
        key_cat[:, :KV_RANK] = lat
        key_cat[:, KV_RANK : KV_RANK + ROPE] = rope
        key_t[...] = lat.T
        for h in range(heads_mla):
            scores = dot_nt(key_cat[...], queries[h]) * scale
            if diagonal:
                key = lax.broadcasted_iota(jnp.int32, scores.shape, 0)
                query = lax.broadcasted_iota(jnp.int32, scores.shape, 1)
                scores = jnp.where(key <= query, scores, MASKED_VALUE)
            old = top[h]
            new = jnp.maximum(old, jnp.max(scores, axis=0, keepdims=True))
            raw = jnp.exp2(scores - new)
            rescale = jnp.exp2(old - new)
            total[h] = total[h] * rescale + jnp.sum(raw, axis=0, keepdims=True)
            acc[h] = acc[h] * rescale + dot_f32(key_t[...], raw.astype(jnp.bfloat16))
            top[h] = new

    def visit(first):
        planes = count // PLANE
        ahead = lax.div(kg.plane, PLANE) - lax.div(first, PLANE) - 1
        size = lax.div(ahead + planes, planes) * PLANE

        @pl.loop(0, size)
        def _(j):
            update(first + j, False)

    kg.partner(0, 3)
    update(me, True)

    @pl.loop(0, me - kg.plane)
    def _(j):
        update(kg.plane + j, False)

    kg.step3()
    kg.partner(3, 4)
    visit(kg.left_plane)
    kg.step4()
    kg.partner(4, 5)
    visit(kg.right_plane)
    kg.partner(5, 6)
    visit(kg.far)

    for h in range(heads_mla):
        latent_out = (acc[h] / total[h]).astype(jnp.bfloat16)
        up = value_up_ref[:, pl.ds(pl.multiple_of((core * heads_mla + h) * VDIM, VDIM), VDIM)]
        mla_all[core, :, h * VDIM : (h + 1) * VDIM] = lax.dot_general(
            latent_out, up, (((0,), (0,)), ((), ())), preferred_element_type=jnp.float32
        ).astype(jnp.bfloat16)
    mla_swap = swap_all(mla_all, 3)
    kg.finish()
    swa_swap.wait()
    for load in out_loads:
        load.wait()
    width_out = heads_mla * VDIM

    def product(values, first):
        width = values.shape[1]
        return dot_f32(values, out_weights[pl.ds(pl.multiple_of(first, width), width), :])

    own_part = (
        product(swa_all[0], out_rows)
        + product(swa_all[1], out_rows + width_swa)
        + product(mla_all[core], core * width_out)
    )
    mla_swap.wait()
    mixed = own_part + product(mla_all[1 - core], (1 - core) * width_out)
    out_ref[...] = mixed.astype(jnp.bfloat16)
    edge.wait_send()
    swap.wait_send()


def fast_shards(
    inputs,
    norm_gain,
    latent_down,
    rope_down,
    latent_gain,
    mla_query,
    key_up,
    value_up,
    swa_query,
    swa_key,
    swa_value,
    sink_logits,
    out_mla,
    out_swa,
):
    count = lax.axis_size("sp")
    cores = lax.axis_size("tp")
    own, depth = inputs.shape
    block = own * cores
    width_mla, width_swa, width_kv = mla_query.shape[1], swa_query.shape[1], swa_key.shape[1]
    heads_mla = width_mla // (NOPE + ROPE)
    width_all = width_mla + width_swa + 2 * width_kv
    inverse = ROPE_BASE ** (-jnp.arange(0, ROPE, 2, dtype=jnp.float32) / ROPE)
    positions = lax.axis_index("sp") * block + jnp.arange(block, dtype=jnp.int32)
    angles = positions.astype(jnp.float32)[:, None] * inverse[None, :]
    down_rows = latent_down.shape[0]
    shard_rows = down_rows // 2 + down_rows // 2 * ROPE // KV_RANK
    key_rows = own + own * ROPE // KV_RANK
    vmem = pl.BlockSpec(memory_space=pltpu.VMEM)
    hbm = pl.BlockSpec(memory_space=pl.ANY)
    bf16 = jnp.bfloat16
    return pl.pallas_call(
        lambda *refs: layer_kernel(count, *refs),
        out_shape=jax.ShapeDtypeStruct((block, out_mla.shape[1]), bf16),
        in_specs=[vmem] * 8
        + [pl.BlockSpec(memory_space=pltpu.SMEM)]
        + [hbm] * 4
        + [vmem]
        + [hbm] * 2,
        out_specs=vmem,
        scratch_shapes=[
            pltpu.VMEM((count, cores, key_rows, KV_RANK), bf16),
            pltpu.VMEM((heads_mla, block, KV_RANK + 2 * ROPE), bf16),
            pltpu.VMEM((block, KV_RANK + 2 * ROPE), bf16),
            pltpu.VMEM((KV_RANK, block), bf16),
            pltpu.VMEM((heads_mla, 1, block), jnp.float32),
            pltpu.VMEM((heads_mla, 1, block), jnp.float32),
            pltpu.VMEM((heads_mla, KV_RANK, block), jnp.float32),
            pltpu.VMEM((cores, block, heads_mla * VDIM), bf16),
            pltpu.VMEM((cores, block, width_swa), bf16),
            pltpu.VMEM((out_mla.shape[0] + out_swa.shape[0], out_mla.shape[1]), bf16),
            pltpu.VMEM((depth, width_all), bf16),
            pltpu.VMEM((block, depth), bf16),
            pltpu.VMEM((block, width_all), bf16),
            pltpu.VMEM((count, cores, shard_rows, KV_RANK), bf16),
            pltpu.VMEM((WINDOW + block, 2 * width_kv), bf16),
            pltpu.SemaphoreType.DMA((6,)),
            pltpu.SemaphoreType.DMA((COPIES,)),
            pltpu.SemaphoreType.DMA((COPIES,)),
            pltpu.SemaphoreType.DMA((COPIES,)),
            pltpu.SemaphoreType.DMA((COPIES,)),
            pltpu.SemaphoreType.DMA((4,)),
            pltpu.SemaphoreType.DMA((4,)),
        ],
        compiler_params=pltpu.CompilerParams(
            collective_id=0, has_side_effects=True, vmem_limit_bytes=56 * 2**20
        ),
        name="layer",
    )(
        inputs,
        norm_gain[None, :],
        latent_down,
        rope_down,
        latent_gain[None, :],
        jnp.cos(angles),
        jnp.sin(angles),
        key_up,
        sink_logits,
        mla_query,
        swa_query,
        swa_key,
        swa_value,
        value_up,
        out_mla,
        out_swa,
    )


def solution(mesh):
    in_specs = (
        P(("sp", "tp"), None),
        P(),
        P("sp", None),
        P("sp", None),
        P(),
        P(None, "tp"),
        P(),
        P(),
        P(None, "tp"),
        P(None, "tp"),
        P(None, "tp"),
        P(),
        P(None, "tp"),
        P(None, "tp"),
    )
    out_specs = P("sp", "tp")
    fast = mesh.shape["tp"] == 2 and mesh.shape["sp"] == 4 * PLANE
    body = fast_shards if fast else shards
    return jax.shard_map(body, mesh=mesh, in_specs=in_specs, out_specs=out_specs, check_vma=False)
```

profile of v0, /device:TPU:25, one launch (start us, length us, event | category | flops | bytes accessed | tf_op | source)
XLA Modules:
  0.0 104.8 jit_solution(13672729816919754434)
XLA Ops:
  0.0 1.4 %copy.17.refs_3_ = bf16[128,64]{1,0:T(8,128)(2,1)} copy(bf16[128,64]{0,1:T(8,128)(2,1)} %param.17) | data formatting | bytes 32768 | tf_op args[3]
  1.5 1.5 %multiply_sine_fusion = (f32[384,32]{1,0:T(8,128)}, f32[384,32]{1,0:T(8,128)}) fusion(f32[384]{0:T(512)S(1)} %add_convert_fusion, f32[32]{0:T(128)S(1)} %multiply_power_fusion), kind=kLoop, calls=%fused_computation | loop fusion | flops 12288 | bytes 99968 | tf_op jit(solution)/shard_map/sin | solution.py:717
  3.0 99.8 %layer.1 = bf16[384,1024]{1,0:T(8,128)(2,1)} custom-call(bf16[192,2048]{1,0:T(8,128)(2,1)} %refs_0_.1, f32[1,2048]{1,0:T(1,128)} %bitcast.2, bf16[128,256]{1,0:T(8,128)(2,1)} %refs_2_.1, bf16[128,64]{1,0:T(8,128)(2,1)} %copy.17.refs_3_, f32[1,256]{1,0:T(1,128)} %bitcast.3, f32[384,32]{1,0:T(8,128)} %get-tuple-element.6.refs_5_, ...), custom_call_target="tpu_custom_call" | custom-call | tf_op jit(solution)/shard_map/layer/pallas_call | solution.py:673
  102.8 2.1 %copy.19 = bf16[384,1024]{1,0:T(8,128)(2,1)} copy(bf16[384,1024]{1,0:T(8,128)(2,1)} %layer.1) | data formatting | bytes 1572864
  (2 shorter events, 0.0 us)
where the time goes:
time: 105 us
  Pallas kernels  99.8 us (95%)
  local copies, waits for them, and re-layouts  3.5 us (3%)
  other arithmetic  1.51 us (1%)
    pallas_call x1, Pallas kernels, fast_shards(): pl.pallas_call(lambda *refs: layer_kernel(count, *refs), out_shape=jax.Sh...  99.8 us
    unnamed x2, local copies, waits for them, and re-layouts  3.5 us

commit v1 on v0

--- a/solution.py
+++ b/solution.py
@@ -1,3 +1,4 @@
+import contextlib
 import math
 
 import jax
@@ -245,8 +246,12 @@
 
 MESH = pl.DeviceIdType.MESH
 LOG2E = 1.4426950408889634
-COPIES = 12
 PLANE = 4
+PLANES = 4
+
+
+def phase(name):
+    return contextlib.nullcontext()
 
 
 def normalize(values, gains):
@@ -277,73 +282,40 @@
     return lax.dot_general(a, b, (((1,), (1,)), ((), ())), preferred_element_type=jnp.float32)
 
 
-class Gather:
-    def __init__(self, buf, send, recv, me, core, count):
-        self.buf, self.send, self.recv, self.core = buf, send, recv, core
-        self.me = me
-        self.x = me + 1 - 2 * lax.rem(me, 2)
-        self.y = me + 2 - 4 * lax.rem(lax.div(me, 2), 2)
-        self.plane = lax.div(me, PLANE) * PLANE
-        self.right = lax.rem(me + PLANE, count)
-        self.left = lax.rem(me + count - PLANE, count)
-        self.right_plane = lax.div(self.right, PLANE) * PLANE
-        self.left_plane = lax.div(self.left, PLANE) * PLANE
-        self.far = lax.rem(self.plane + 2 * PLANE, count)
+class Sends:
+    def __init__(self, core):
+        self.core = core
         self.started = []
 
-    def go(self, index, first, size, device):
-        part = self.buf.at[pl.ds(first, size), pl.ds(self.core, 1)]
-        copy = pltpu.make_async_remote_copy(
+    def copy(self, part, device, send, recv):
+        return pltpu.make_async_remote_copy(
             src_ref=part,
             dst_ref=part,
-            send_sem=self.send.at[index],
-            recv_sem=self.recv.at[index],
+            send_sem=send,
+            recv_sem=recv,
             device_id=device,
             device_id_type=MESH,
         )
-        copy.start()
-        self.started.append(copy)
+
+    def go(self, part, device, send, recv, cond=None):
+        copy = self.copy(part, device, send, recv)
+        if cond is None:
+            copy.start()
+        else:
+            pl.when(cond)(lambda: copy.start())
+        self.started.append((copy, cond))
         return copy
 
-    def pair(self, index, first, size):
-        return self.go(index, first, size, {"tp": 1 - self.core})
-
-    def step0(self):
-        self.cx = self.go(0, self.me, 1, {"sp": self.x})
-        self.p = [self.pair(6, self.me, 1)]
-
-    def step1(self):
-        self.cx.wait_recv()
-        self.cy = self.go(1, lax.div(self.me, 2) * 2, 2, {"sp": self.y})
-        self.p.append(self.pair(7, self.x, 1))
-
-    def step2(self):
-        self.cy.wait_recv()
-        self.cr = self.go(2, self.plane, PLANE, {"sp": self.right})
-        self.cl = self.go(3, self.plane, PLANE, {"sp": self.left})
-        self.p.append(self.pair(8, lax.div(self.y, 2) * 2, 2))
-
-    def step3(self):
-        half = PLANE // 2
-        self.cr.wait_recv()
-        self.rr = self.go(4, self.left_plane, half, {"sp": self.right})
-        self.p.append(self.pair(9, self.left_plane, PLANE))
-        self.cl.wait_recv()
-        self.rl = self.go(5, self.right_plane + half, half, {"sp": self.left})
-        self.p.append(self.pair(10, self.right_plane, PLANE))
-
-    def step4(self):
-        self.rr.wait_recv()
-        self.rl.wait_recv()
-        self.p.append(self.pair(11, self.far, PLANE))
-
-    def partner(self, first, last):
-        for copy in self.p[first:last]:
-            copy.wait_recv()
+    def pair(self, part, send, recv):
+        return self.copy(part, {"tp": 1 - self.core}, send, recv)
 
     def finish(self):
-        for copy in self.started:
-            copy.wait_send()
+        for copy, cond in self.started:
+            if cond is None:
+                copy.wait_send()
+            else:
+                pl.when(cond)(lambda copy=copy: copy.wait_send())
+        self.started = []
 
 
 def layer_kernel(
@@ -383,13 +355,19 @@
     local_sem,
     wsend,
     wrecv,
+    wtsend,
+    wtrecv,
     ksend,
     krecv,
+    ktsend,
+    ktrecv,
     xsend,
     xrecv,
 ):
     me = lax.axis_index("sp")
     core = lax.axis_index("tp")
+    z, c = lax.div(me, PLANE), lax.rem(me, PLANE)
+    cx, cy = lax.rem(c, 2), lax.div(c, 2)
     own = x_ref.shape[0]
     block = 2 * own
     width_mla = wq_ref.shape[1]
@@ -399,6 +377,16 @@
     heads_swa = width_swa // HEAD
     group = width_swa // width_kv
     half_down = down_ref.shape[0] // 2
+    others = (
+        jnp.where(z == 0, 1, z - 1),
+        jnp.where(z == 0, 2, jnp.where(z == PLANES - 1, 1, z + 1)),
+        jnp.where(z < 2, 3, 0),
+    )
+
+    def column(q):
+        return lax.rem(cy + lax.div(q, 2), 2) * 2 + lax.rem(cx + lax.rem(q, 2), 2)
+
+    beside = [z * PLANE + column(jnp.int32(q)) for q in range(1, PLANE)]
 
     loads, start = [], 0
     for i, ref in enumerate((wq_ref, wsq_ref, wsk_ref, wsv_ref)):
@@ -421,40 +409,66 @@
     gathered[me, core, :half_down, :] = down_ref[rows, :]
     gathered[me, core, half_down:, :] = pack_rope(rope_down_ref[rows, :])
 
-    wg = Gather(gathered, wsend, wrecv, me, core, count)
-    kg = Gather(keys_ref, ksend, krecv, me, core, count)
-    after = lax.rem(me + 1, count)
-    before = lax.rem(me + count - 1, count)
+    sends = Sends(core)
     barrier = pltpu.get_barrier_semaphore()
-    devices = [{"sp": d} for d in (wg.x, wg.y, wg.right, wg.left, after, before)]
+    devices = [{"sp": d} for d in beside]
+    devices += [{"sp": zz * PLANE + c} for zz in others]
     devices.append({"tp": 1 - core})
+    has_after = jnp.logical_and(c == PLANE - 1, z < PLANES - 1)
+    has_before = jnp.logical_and(c == 0, z > 0)
+
+    def greet(device):
+        pl.semaphore_signal(barrier, inc=1, device_id=device, device_id_type=MESH)
+
     for device in devices:
-        pl.semaphore_signal(barrier, inc=1, device_id=device, device_id_type=MESH)
-    pl.semaphore_wait(barrier, len(devices))
-    wg.step0()
+        greet(device)
+    pl.when(has_after)(lambda: greet({"sp": me + 1}))
+    pl.when(has_before)(lambda: greet({"sp": me - 1}))
+    with phase("w_barrier"):
+        extra = jnp.where(jnp.logical_or(has_after, has_before), 1, 0)
+        pl.semaphore_wait(barrier, len(devices) + extra)
+
+    def shard(j):
+        return gathered.at[pl.ds(j, 1), pl.ds(core, 1)]
+
+    for d in range(PLANES - 1, 0, -1):
+        for k, step in enumerate((d, -d)):
+            cond = (z + step < PLANES) if step > 0 else (z + step >= 0)
+            sends.go(
+                shard(me),
+                {"sp": me + step * PLANE},
+                wsend.at[2 * (d - 1) + k],
+                wrecv.at[me],
+                cond,
+            )
+
+    def spread(j, level):
+        for q in range(PLANE - 1):
+            sends.go(
+                shard(j), {"sp": beside[q]}, wsend.at[6 + 3 * level + q], wrecv.at[j]
+            )
+
+    spread(me, 0)
 
     mine = pl.multiple_of(core * own, own)
     other = pl.multiple_of((1 - core) * own, own)
     chunk = 32
 
-    @pl.loop(0, own // chunk)
-    def _(i):
-        at = pl.multiple_of(i * chunk, chunk)
-        normed[pl.ds(mine + at, chunk), :] = normalize(x_ref[pl.ds(at, chunk), :], gain_ref[...])
-
-    part = normed.at[pl.ds(mine, own)]
-    swap = pltpu.make_async_remote_copy(
-        src_ref=part,
-        dst_ref=part,
-        send_sem=xsend.at[0],
-        recv_sem=xrecv.at[0],
-        device_id={"tp": 1 - core},
-        device_id_type=MESH,
-    )
-    swap.start()
-    wg.step1()
-    for load in loads:
-        load.wait()
+    with phase("norm"):
+
+        @pl.loop(0, own // chunk)
+        def _(i):
+            at = pl.multiple_of(i * chunk, chunk)
+            normed[pl.ds(mine + at, chunk), :] = normalize(
+                x_ref[pl.ds(at, chunk), :], gain_ref[...]
+            )
+
+    swap = sends.go(
+        normed.at[pl.ds(mine, own)], {"tp": 1 - core}, xsend.at[0], xrecv.at[0]
+    )
+    with phase("w_loads"):
+        for load in loads:
+            load.wait()
 
     for load in out_loads:
         load.start()
@@ -466,58 +480,73 @@
                 jnp.bfloat16
             )
 
-    wg.step2()
-    project(mine)
-    wg.step3()
-    swap.wait_recv()
-    project(other)
-    wg.step4()
+    def arrived(part, recv):
+        sends.pair(part, xsend.at[0], recv).wait_recv()
+
+    with phase("proj1"):
+        project(mine)
+    for level, zz in enumerate(others):
+        with phase("w_z"):
+            arrived(shard(zz * PLANE + c), wrecv.at[zz * PLANE + c])
+        spread(zz * PLANE + c, level + 1)
+    with phase("w_swap"):
+        swap.wait_recv()
+    with phase("proj2"):
+        project(other)
 
     kv = width_mla + width_swa
     window[WINDOW:, :] = proj[:, kv:]
+    has_next, has_last = me < count - 1, me > 0
+    edge_rows = window.at[pl.ds(block, WINDOW)]
     edge = pltpu.make_async_remote_copy(
-        src_ref=window.at[pl.ds(block, WINDOW)],
+        src_ref=edge_rows,
         dst_ref=window.at[pl.ds(0, WINDOW)],
         send_sem=xsend.at[1],
         recv_sem=xrecv.at[1],
-        device_id={"sp": after},
+        device_id={"sp": jnp.minimum(me + 1, count - 1)},
         device_id_type=MESH,
     )
-    edge.start()
-    queries[...] = jnp.zeros_like(queries)
-    key_cat[...] = jnp.zeros_like(key_cat)
-    cos, sin = cos_ref[...], sin_ref[...]
-    for h in range(heads_mla):
-        base = h * (NOPE + ROPE)
-        up = key_up_ref[:, pl.ds(pl.multiple_of((core * heads_mla + h) * NOPE, NOPE), NOPE)]
-        queries[h, :, :KV_RANK] = dot_nt(proj[:, base : base + NOPE], up).astype(jnp.bfloat16)
-        queries[h, :, KV_RANK : KV_RANK + ROPE] = turn(proj[:, base + NOPE : base + NOPE + ROPE], cos, sin)
-    wg.partner(0, 6)
-    wg.finish()
-
-    lhs = normed[pl.ds(mine, own), :]
-    depth = lhs.shape[1]
-    down = gathered[:, :, :half_down, :].reshape(depth, KV_RANK)
-    packed = gathered[:, :, half_down:, :]
-    rope_down = jnp.concatenate(
-        [packed[:, :, :, g * ROPE : (g + 1) * ROPE] for g in range(4)], axis=2
-    ).reshape(depth, ROPE)
-    latent = dot_f32(lhs, down).astype(jnp.bfloat16)
-    rope_raw = dot_f32(lhs, rope_down).astype(jnp.bfloat16)
-    keys_ref[me, core, :own, :] = normalize(latent, latent_gain_ref[...])
-    keys_rope = turn(rope_raw, cos_ref[pl.ds(mine, own), :], sin_ref[pl.ds(mine, own), :])
-    keys_ref[me, core, own:, :] = pack_rope(keys_rope)
-    kg.step0()
+
+    @pl.when(has_next)
+    def _():
+        edge.start()
+
+    @pl.when(me == 0)
+    def _():
+        window[:WINDOW, :] = jnp.zeros_like(window[:WINDOW, :])
+
+    def hand_over(zz, level):
+        with phase("w_plane"):
+            for q in range(1, PLANE):
+                j = zz * PLANE + column(jnp.int32(q))
+                arrived(shard(j), wrecv.at[j])
+        part = gathered.at[pl.ds(zz * PLANE, PLANE), pl.ds(core, 1)]
+        return sends.go(part, {"tp": 1 - core}, wtsend.at[level], wtrecv.at[zz])
+
+    handed = [hand_over(z, 0)]
+    with phase("queries"):
+        queries[...] = jnp.zeros_like(queries)
+        key_cat[...] = jnp.zeros_like(key_cat)
+        cos, sin = cos_ref[...], sin_ref[...]
+        for h in range(heads_mla):
+            base = h * (NOPE + ROPE)
+            up = key_up_ref[:, pl.ds(pl.multiple_of((core * heads_mla + h) * NOPE, NOPE), NOPE)]
+            queries[h, :, :KV_RANK] = dot_nt(proj[:, base : base + NOPE], up).astype(jnp.bfloat16)
+            queries[h, :, KV_RANK : KV_RANK + ROPE] = turn(
+                proj[:, base + NOPE : base + NOPE + ROPE], cos, sin
+            )
+    for level, zz in enumerate(others):
+        handed.append(hand_over(zz, level + 1))
 
     row = lax.broadcasted_iota(jnp.int32, (WINDOW, 2 * WINDOW), 0)
-    column = lax.broadcasted_iota(jnp.int32, (WINDOW, 2 * WINDOW), 1)
-    distance = row + WINDOW - column
+    column_of = lax.broadcasted_iota(jnp.int32, (WINDOW, 2 * WINDOW), 1)
+    distance = row + WINDOW - column_of
     inside = (distance >= 0) & (distance < WINDOW)
 
     def windowed(tile):
         allowed = inside
         if tile == 0:
-            allowed = inside & ((column >= WINDOW) | (me > 0))
+            allowed = inside & ((column_of >= WINDOW) | (me > 0))
         at = tile * WINDOW
         outs = []
         for h in range(heads_swa):
@@ -533,27 +562,82 @@
             outs.append(dot_f32((raw / total).astype(jnp.bfloat16), v).astype(jnp.bfloat16))
         swa_all[core, at : at + WINDOW, :] = jnp.concatenate(outs, axis=1)
 
+    with phase("w_handed"):
+        for copy in handed:
+            copy.wait_recv()
+        sends.finish()
+
+    with phase("latent"):
+        lhs = normed[pl.ds(mine, own), :]
+        depth = lhs.shape[1]
+        down = gathered[:, :, :half_down, :].reshape(depth, KV_RANK)
+        packed = gathered[:, :, half_down:, :]
+        rope_down = jnp.concatenate(
+            [packed[:, :, :, g * ROPE : (g + 1) * ROPE] for g in range(4)], axis=2
+        ).reshape(depth, ROPE)
+        latent = dot_f32(lhs, down).astype(jnp.bfloat16)
+        rope_raw = dot_f32(lhs, rope_down).astype(jnp.bfloat16)
+        keys_ref[me, core, :own, :] = normalize(latent, latent_gain_ref[...])
+        keys_rope = turn(rope_raw, cos_ref[pl.ds(mine, own), :], sin_ref[pl.ds(mine, own), :])
+        keys_ref[me, core, own:, :] = pack_rope(keys_rope)
+
+    def key(j):
+        return keys_ref.at[pl.ds(j, 1), pl.ds(core, 1)]
+
+    for d in range(PLANES - 1, 0, -1):
+        sends.go(
+            key(me), {"sp": me + d * PLANE}, ksend.at[d - 1], krecv.at[me], z + d < PLANES
+        )
+
+    def spread_keys(j, level, conds):
+        for q in range(PLANE - 1):
+            sends.go(
+                key(j), {"sp": beside[q]}, ksend.at[3 + 3 * level + q], krecv.at[j], conds[q]
+            )
+
+    def pass_on(j):
+        sends.pair(key(j), ktsend.at[j], ktrecv.at[j]).start()
+
+    spread_keys(me, 0, (cx == 0, cy == 0, cy == 0))
+    pass_on(me)
+
+    def block_at(n):
+        later = jnp.maximum(n - c - 1, 0)
+        q = lax.rem(later, PLANE)
+        j = (z - lax.div(later, PLANE) - 1) * PLANE + column(q)
+        first = jnp.logical_and(n > c, q == 0)
+        return jnp.where(n <= c, me - n, j), first
+
+    def fetch(n):
+        j, first = block_at(n)
+
+        @pl.when(jnp.logical_and(n <= me, jnp.logical_not(first)))
+        def _():
+            arrived(key(j), krecv.at[j])
+            pass_on(j)
+
+    def lift(d):
+        j = (z - d) * PLANE + c
+
+        @pl.when(z >= d)
+        def _():
+            arrived(key(j), krecv.at[j])
+            pass_on(j)
+
+        spread_keys(j, d, (z >= d,) * 3)
+
     def swap_all(buf, index):
-        part = buf.at[pl.ds(core, 1)]
-        copy = pltpu.make_async_remote_copy(
-            src_ref=part,
-            dst_ref=part,
-            send_sem=xsend.at[index],
-            recv_sem=xrecv.at[index],
-            device_id={"tp": 1 - core},
-            device_id_type=MESH,
+        return sends.go(
+            buf.at[pl.ds(core, 1)], {"tp": 1 - core}, xsend.at[index], xrecv.at[index]
         )
-        copy.start()
-        return copy
-
-    for tile in range(1, 2):
-        windowed(tile)
-    kg.step1()
-    for tile in range(2, block // WINDOW):
-        windowed(tile)
-    edge.wait_recv()
-    windowed(0)
-    kg.step2()
+
+    with phase("win12"):
+        for tile in range(1, block // WINDOW):
+            windowed(tile)
+    with phase("w_edge"):
+        pl.when(has_last)(lambda: edge.wait_recv())
+    with phase("win0"):
+        windowed(0)
     swa_swap = swap_all(swa_all, 2)
 
     top[...] = jnp.full_like(top, MASKED_VALUE)
@@ -573,9 +657,9 @@
         for h in range(heads_mla):
             scores = dot_nt(key_cat[...], queries[h]) * scale
             if diagonal:
-                key = lax.broadcasted_iota(jnp.int32, scores.shape, 0)
-                query = lax.broadcasted_iota(jnp.int32, scores.shape, 1)
-                scores = jnp.where(key <= query, scores, MASKED_VALUE)
+                key_at = lax.broadcasted_iota(jnp.int32, scores.shape, 0)
+                query_at = lax.broadcasted_iota(jnp.int32, scores.shape, 1)
+                scores = jnp.where(key_at <= query_at, scores, MASKED_VALUE)
             old = top[h]
             new = jnp.maximum(old, jnp.max(scores, axis=0, keepdims=True))
             raw = jnp.exp2(scores - new)
@@ -584,58 +668,81 @@
             acc[h] = acc[h] * rescale + dot_f32(key_t[...], raw.astype(jnp.bfloat16))
             top[h] = new
 
-    def visit(first):
-        planes = count // PLANE
-        ahead = lax.div(kg.plane, PLANE) - lax.div(first, PLANE) - 1
-        size = lax.div(ahead + planes, planes) * PLANE
-
-        @pl.loop(0, size)
-        def _(j):
-            update(first + j, False)
-
-    kg.partner(0, 3)
-    update(me, True)
-
-    @pl.loop(0, me - kg.plane)
-    def _(j):
-        update(kg.plane + j, False)
-
-    kg.step3()
-    kg.partner(3, 4)
-    visit(kg.left_plane)
-    kg.step4()
-    kg.partner(4, 5)
-    visit(kg.right_plane)
-    kg.partner(5, 6)
-    visit(kg.far)
-
-    for h in range(heads_mla):
-        latent_out = (acc[h] / total[h]).astype(jnp.bfloat16)
-        up = value_up_ref[:, pl.ds(pl.multiple_of((core * heads_mla + h) * VDIM, VDIM), VDIM)]
-        mla_all[core, :, h * VDIM : (h + 1) * VDIM] = lax.dot_general(
-            latent_out, up, (((0,), (0,)), ((), ())), preferred_element_type=jnp.float32
-        ).astype(jnp.bfloat16)
+    with phase("w_lift1"):
+        lift(1)
+        fetch(jnp.int32(1))
+    with phase("w_own"):
+        sends.pair(key(me), ktsend.at[me], ktrecv.at[me]).wait_recv()
+    with phase("diag"):
+        update(me, True)
+
+    def step(n):
+        j, _ = block_at(n)
+        with phase("w_fetch"):
+            fetch(n + 1)
+        with phase("w_pair"):
+            sends.pair(key(j), ktsend.at[j], ktrecv.at[j]).wait_recv()
+        with phase("update"):
+            update(j, False)
+
+    with phase("loop1"):
+        step_end = jnp.minimum(me + 1, 2)
+
+        @pl.loop(1, step_end)
+        def _(n):
+            step(n)
+
+    with phase("w_lift2"):
+        lift(2)
+    with phase("loop2"):
+
+        @pl.loop(2, jnp.minimum(me + 1, 3))
+        def _(n):
+            step(n)
+
+    with phase("w_lift3"):
+        lift(3)
+    with phase("loop3"):
+
+        @pl.loop(3, me + 1)
+        def _(n):
+            step(n)
+
+    with phase("value_up"):
+        for h in range(heads_mla):
+            latent_out = (acc[h] / total[h]).astype(jnp.bfloat16)
+            up = value_up_ref[:, pl.ds(pl.multiple_of((core * heads_mla + h) * VDIM, VDIM), VDIM)]
+            mla_all[core, :, h * VDIM : (h + 1) * VDIM] = lax.dot_general(
+                latent_out, up, (((0,), (0,)), ((), ())), preferred_element_type=jnp.float32
+            ).astype(jnp.bfloat16)
     mla_swap = swap_all(mla_all, 3)
-    kg.finish()
-    swa_swap.wait()
-    for load in out_loads:
-        load.wait()
+    with phase("w_finish"):
+        swa_swap.wait_recv()
+        for load in out_loads:
+            load.wait()
     width_out = heads_mla * VDIM
 
     def product(values, first):
         width = values.shape[1]
         return dot_f32(values, out_weights[pl.ds(pl.multiple_of(first, width), width), :])
 
-    own_part = (
-        product(swa_all[0], out_rows)
-        + product(swa_all[1], out_rows + width_swa)
-        + product(mla_all[core], core * width_out)
-    )
-    mla_swap.wait()
-    mixed = own_part + product(mla_all[1 - core], (1 - core) * width_out)
-    out_ref[...] = mixed.astype(jnp.bfloat16)
-    edge.wait_send()
-    swap.wait_send()
+    with phase("out1"):
+        own_part = (
+            product(swa_all[0], out_rows)
+            + product(swa_all[1], out_rows + width_swa)
+            + product(mla_all[core], core * width_out)
+        )
+    with phase("w_mlaswap"):
+        mla_swap.wait_recv()
+    with phase("out2"):
+        mixed = own_part + product(mla_all[1 - core], (1 - core) * width_out)
+        out_ref[...] = mixed.astype(jnp.bfloat16)
+    sends.finish()
+    pl.when(has_next)(lambda: edge.wait_send())
+
+    @pl.loop(0, me + 1)
+    def _(j):
+        sends.pair(key(j), ktsend.at[j], ktrecv.at[j]).wait_send()
 
 
 def fast_shards(
@@ -696,10 +803,14 @@
             pltpu.VMEM((count, cores, shard_rows, KV_RANK), bf16),
             pltpu.VMEM((WINDOW + block, 2 * width_kv), bf16),
             pltpu.SemaphoreType.DMA((6,)),
-            pltpu.SemaphoreType.DMA((COPIES,)),
-            pltpu.SemaphoreType.DMA((COPIES,)),
-            pltpu.SemaphoreType.DMA((COPIES,)),
-            pltpu.SemaphoreType.DMA((COPIES,)),
+            pltpu.SemaphoreType.DMA((6 + 3 * PLANES,)),
+            pltpu.SemaphoreType.DMA((count,)),
+            pltpu.SemaphoreType.DMA((PLANES,)),
+            pltpu.SemaphoreType.DMA((PLANES,)),
+            pltpu.SemaphoreType.DMA((3 + 3 * PLANES,)),
+            pltpu.SemaphoreType.DMA((count,)),
+            pltpu.SemaphoreType.DMA((count,)),
+            pltpu.SemaphoreType.DMA((count,)),
             pltpu.SemaphoreType.DMA((4,)),
             pltpu.SemaphoreType.DMA((4,)),
         ],
@@ -745,6 +856,6 @@
         P(None, "tp"),
     )
     out_specs = P("sp", "tp")
-    fast = mesh.shape["tp"] == 2 and mesh.shape["sp"] == 4 * PLANE
+    fast = mesh.shape["tp"] == 2 and mesh.shape["sp"] == PLANES * PLANE
     body = fast_shards if fast else shards
     return jax.shard_map(body, mesh=mesh, in_specs=in_specs, out_specs=out_specs, check_vma=False)

time: 105 us -> 73.2 us (0.70)
  the two profiles are of different devices: /device:TPU:25 before, /device:TPU:31 now
where the time goes in v1:
time: 73.2 us; the launch traced here: 73 us
  Pallas kernels  67.9 us (93%)
  local copies, waits for them, and re-layouts  3.5 us (5%)
  other arithmetic  1.51 us (2%)
    pallas_call x1, Pallas kernels, fast_shards(): pl.pallas_call(lambda *refs: layer_kernel(count, *refs), out_shape=jax.Sh...  67.9 us
    unnamed x2, local copies, waits for them, and re-layouts  3.5 us
    sin x1, other arithmetic, fast_shards(): jnp.sin(angles)  1.5 us

profile of v1, /device:TPU:31, one launch (start us, length us, event | category | flops | bytes accessed | tf_op | source)
XLA Modules:
  0.0 73.0 jit_solution(17828681086961281291)
XLA Ops:
  0.0 1.4 %copy.17.refs_3_ = bf16[128,64]{1,0:T(8,128)(2,1)} copy(bf16[128,64]{0,1:T(8,128)(2,1)} %param.17) | data formatting | bytes 32768 | tf_op args[3]
  1.5 1.5 %multiply_sine_fusion = (f32[384,32]{1,0:T(8,128)}, f32[384,32]{1,0:T(8,128)}) fusion(f32[384]{0:T(512)S(1)} %add_convert_fusion, f32[32]{0:T(128)S(1)} %multiply_power_fusion), kind=kLoop, calls=%fused_computation | loop fusion | flops 12288 | bytes 99968 | tf_op jit(solution)/shard_map/sin | solution.py:828
  3.0 67.9 %layer.1 = bf16[384,1024]{1,0:T(8,128)(2,1)} custom-call(bf16[192,2048]{1,0:T(8,128)(2,1)} %refs_0_.1, f32[1,2048]{1,0:T(1,128)} %bitcast.2, bf16[128,256]{1,0:T(8,128)(2,1)} %refs_2_.1, bf16[128,64]{1,0:T(8,128)(2,1)} %copy.17.refs_3_, f32[1,256]{1,0:T(1,128)} %bitcast.3, f32[384,32]{1,0:T(8,128)} %get-tuple-element.6.refs_5_, ...), custom_call_target="tpu_custom_call" | custom-call | tf_op jit(solution)/shard_map/layer/pallas_call | solution.py:780
  70.9 2.1 %copy.19 = bf16[384,1024]{1,0:T(8,128)(2,1)} copy(bf16[384,1024]{1,0:T(8,128)(2,1)} %layer.1) | data formatting | bytes 1572864
  (2 shorter events, 0.0 us)

commit v2 on v1

--- a/solution.py
+++ b/solution.py
@@ -3,6 +3,7 @@
 
 import jax
 import jax.numpy as jnp
+import numpy as np
 from jax import lax
 from jax.experimental import pallas as pl
 from jax.experimental.pallas import tpu as pltpu
@@ -320,23 +321,35 @@
 
 def layer_kernel(
     count,
-    x_ref,
-    gain_ref,
-    down_ref,
-    rope_down_ref,
-    latent_gain_ref,
-    cos_ref,
-    sin_ref,
-    key_up_ref,
-    sink_ref,
+    x_hbm,
+    gain_hbm,
+    down_hbm,
+    rope_down_hbm,
+    latent_gain_hbm,
+    turns_hbm,
+    bases_hbm,
+    key_up_hbm,
+    sink_hbm,
     wq_ref,
     wsq_ref,
     wsk_ref,
     wsv_ref,
-    value_up_ref,
+    value_up_hbm,
     out_mla_ref,
     out_swa_ref,
     out_ref,
+    x_ref,
+    gain_ref,
+    rope_down_ref,
+    latent_gain_ref,
+    turns_ref,
+    base_ref,
+    key_up_ref,
+    sink_ref,
+    value_up_ref,
+    cos_ref,
+    sin_ref,
+    rope_t,
     keys_ref,
     queries,
     key_cat,
@@ -376,7 +389,9 @@
     heads_mla = width_mla // (NOPE + ROPE)
     heads_swa = width_swa // HEAD
     group = width_swa // width_kv
-    half_down = down_ref.shape[0] // 2
+    half_down = down_hbm.shape[0] // 2
+    columns = heads_mla * block
+    width = math.gcd(columns, 512)
     others = (
         jnp.where(z == 0, 1, z - 1),
         jnp.where(z == 0, 2, jnp.where(z == PLANES - 1, 1, z + 1)),
@@ -387,27 +402,6 @@
         return lax.rem(cy + lax.div(q, 2), 2) * 2 + lax.rem(cx + lax.rem(q, 2), 2)
 
     beside = [z * PLANE + column(jnp.int32(q)) for q in range(1, PLANE)]
-
-    loads, start = [], 0
-    for i, ref in enumerate((wq_ref, wsq_ref, wsk_ref, wsv_ref)):
-        width = ref.shape[1]
-        loads.append(
-            pltpu.make_async_copy(ref, weights.at[:, pl.ds(start, width)], local_sem.at[i])
-        )
-        loads[-1].start()
-        start += width
-    out_rows = out_mla_ref.shape[0]
-    out_loads = []
-    for i, ref in enumerate((out_mla_ref, out_swa_ref)):
-        out_loads.append(
-            pltpu.make_async_copy(
-                ref, out_weights.at[pl.ds(i * out_rows, out_rows)], local_sem.at[4 + i]
-            )
-        )
-
-    rows = pl.ds(pl.multiple_of(core * half_down, half_down), half_down)
-    gathered[me, core, :half_down, :] = down_ref[rows, :]
-    gathered[me, core, half_down:, :] = pack_rope(rope_down_ref[rows, :])
 
     sends = Sends(core)
     barrier = pltpu.get_barrier_semaphore()
@@ -424,6 +418,48 @@
         greet(device)
     pl.when(has_after)(lambda: greet({"sp": me + 1}))
     pl.when(has_before)(lambda: greet({"sp": me - 1}))
+
+    pending = []
+
+    def load(src, dst):
+        copy = pltpu.make_async_copy(src, dst, local_sem.at[len(pending)])
+        pending.append(copy)
+        return copy
+
+    rows = pl.ds(pl.multiple_of(core * half_down, half_down), half_down)
+    early = [
+        load(down_hbm.at[rows], gathered.at[me, core, pl.ds(0, half_down)]),
+        load(rope_down_hbm, rope_down_ref),
+        load(x_hbm, x_ref),
+        load(gain_hbm, gain_ref),
+    ]
+    start = 0
+    loads = []
+    for ref in (wq_ref, wsq_ref, wsk_ref, wsv_ref):
+        loads.append(load(ref, weights.at[:, pl.ds(start, ref.shape[1])]))
+        start += ref.shape[1]
+    small = [
+        load(turns_hbm, turns_ref),
+        load(bases_hbm.at[me], base_ref),
+        load(key_up_hbm, key_up_ref),
+        load(latent_gain_hbm, latent_gain_ref),
+        load(sink_hbm, sink_ref),
+    ]
+    out_rows = out_mla_ref.shape[0]
+    out_loads = [load(value_up_hbm, value_up_ref)]
+    for i, ref in enumerate((out_mla_ref, out_swa_ref)):
+        out_loads.append(load(ref, out_weights.at[pl.ds(i * out_rows, out_rows)]))
+    for copy in early + loads + small:
+        copy.start()
+
+    with phase("w_first"):
+        for copy in early[:2]:
+            copy.wait()
+    piece = half_down * ROPE // KV_RANK
+    at = pl.multiple_of(core * 2 * piece, 2 * piece)
+    gathered[me, core, half_down:, :] = jnp.concatenate(
+        [rope_down_ref[pl.ds(at, piece), :], rope_down_ref[pl.ds(at + piece, piece), :]], axis=1
+    )
     with phase("w_barrier"):
         extra = jnp.where(jnp.logical_or(has_after, has_before), 1, 0)
         pl.semaphore_wait(barrier, len(devices) + extra)
@@ -450,6 +486,9 @@
 
     spread(me, 0)
 
+    with phase("w_x"):
+        for copy in early[2:]:
+            copy.wait()
     mine = pl.multiple_of(core * own, own)
     other = pl.multiple_of((1 - core) * own, own)
     chunk = 32
@@ -467,11 +506,11 @@
         normed.at[pl.ds(mine, own)], {"tp": 1 - core}, xsend.at[0], xrecv.at[0]
     )
     with phase("w_loads"):
-        for load in loads:
-            load.wait()
-
-    for load in out_loads:
-        load.start()
+        for copy in loads:
+            copy.wait()
+
+    for copy in out_loads:
+        copy.start()
 
     def project(at):
         lhs = normed[pl.ds(at, own), :]
@@ -525,16 +564,24 @@
 
     handed = [hand_over(z, 0)]
     with phase("queries"):
-        queries[...] = jnp.zeros_like(queries)
+        for copy in small:
+            copy.wait()
         key_cat[...] = jnp.zeros_like(key_cat)
-        cos, sin = cos_ref[...], sin_ref[...]
+        queries[KV_RANK + ROPE :, :] = jnp.zeros_like(queries[KV_RANK + ROPE :, :])
+        half = ROPE // 2
+        base_cos, base_sin = base_ref[:, :half], base_ref[:, half:]
+        near_cos, near_sin = turns_ref[:, :half], turns_ref[:, half:]
+        cos = base_cos * near_cos - base_sin * near_sin
+        sin = base_sin * near_cos + base_cos * near_sin
+        cos_ref[...], sin_ref[...] = cos, sin
         for h in range(heads_mla):
             base = h * (NOPE + ROPE)
             up = key_up_ref[:, pl.ds(pl.multiple_of((core * heads_mla + h) * NOPE, NOPE), NOPE)]
-            queries[h, :, :KV_RANK] = dot_nt(proj[:, base : base + NOPE], up).astype(jnp.bfloat16)
-            queries[h, :, KV_RANK : KV_RANK + ROPE] = turn(
+            span = slice(h * block, (h + 1) * block)
+            queries[:KV_RANK, span] = dot_nt(up, proj[:, base : base + NOPE]).astype(jnp.bfloat16)
+            queries[KV_RANK : KV_RANK + ROPE, span] = turn(
                 proj[:, base + NOPE : base + NOPE + ROPE], cos, sin
-            )
+            ).T
     for level, zz in enumerate(others):
         handed.append(hand_over(zz, level + 1))
 
@@ -571,12 +618,18 @@
         lhs = normed[pl.ds(mine, own), :]
         depth = lhs.shape[1]
         down = gathered[:, :, :half_down, :].reshape(depth, KV_RANK)
-        packed = gathered[:, :, half_down:, :]
-        rope_down = jnp.concatenate(
-            [packed[:, :, :, g * ROPE : (g + 1) * ROPE] for g in range(4)], axis=2
-        ).reshape(depth, ROPE)
+        for j in range(count):
+            packed = gathered[j, :, half_down:, :]
+            rope_t[:, j * 2 * half_down : (j + 1) * 2 * half_down] = jnp.concatenate(
+                [
+                    packed[k, :, g * 2 * half_down : (g + 1) * 2 * half_down]
+                    for k in range(2)
+                    for g in range(2)
+                ],
+                axis=0,
+            )
         latent = dot_f32(lhs, down).astype(jnp.bfloat16)
-        rope_raw = dot_f32(lhs, rope_down).astype(jnp.bfloat16)
+        rope_raw = dot_nt(lhs, rope_t[...]).astype(jnp.bfloat16)
         keys_ref[me, core, :own, :] = normalize(latent, latent_gain_ref[...])
         keys_rope = turn(rope_raw, cos_ref[pl.ds(mine, own), :], sin_ref[pl.ds(mine, own), :])
         keys_ref[me, core, own:, :] = pack_rope(keys_rope)
@@ -584,21 +637,25 @@
     def key(j):
         return keys_ref.at[pl.ds(j, 1), pl.ds(core, 1)]
 
-    for d in range(PLANES - 1, 0, -1):
+    def raise_own(d):
         sends.go(
             key(me), {"sp": me + d * PLANE}, ksend.at[d - 1], krecv.at[me], z + d < PLANES
         )
 
-    def spread_keys(j, level, conds):
-        for q in range(PLANE - 1):
-            sends.go(
-                key(j), {"sp": beside[q]}, ksend.at[3 + 3 * level + q], krecv.at[j], conds[q]
-            )
+    raise_own(1)
+
+    def beside_keys(j, level):
+        return [
+            sends.copy(key(j), {"sp": beside[q]}, ksend.at[3 + 3 * level + q], krecv.at[j])
+            for q in range(PLANE - 1)
+        ]
 
     def pass_on(j):
         sends.pair(key(j), ktsend.at[j], ktrecv.at[j]).start()
 
-    spread_keys(me, 0, (cx == 0, cy == 0, cy == 0))
+    own_conds = (cx == 0, cy == 0, cy == 0)
+    for copy, cond in zip(beside_keys(me, 0), own_conds):
+        pl.when(cond)(lambda copy=copy: copy.start())
     pass_on(me)
 
     def block_at(n):
@@ -617,14 +674,13 @@
             pass_on(j)
 
     def lift(d):
-        j = (z - d) * PLANE + c
-
         @pl.when(z >= d)
         def _():
+            j = (z - d) * PLANE + c
             arrived(key(j), krecv.at[j])
+            for copy in beside_keys(j, d):
+                copy.start()
             pass_on(j)
-
-        spread_keys(j, d, (z >= d,) * 3)
 
     def swap_all(buf, index):
         return sends.go(
@@ -634,6 +690,7 @@
     with phase("win12"):
         for tile in range(1, block // WINDOW):
             windowed(tile)
+    raise_own(2)
     with phase("w_edge"):
         pl.when(has_last)(lambda: edge.wait_recv())
     with phase("win0"):
@@ -645,72 +702,109 @@
     acc[...] = jnp.zeros_like(acc)
     scale = (NOPE + ROPE) ** (-0.5) * LOG2E
 
-    def update(j, diagonal):
+    def unpack(j, slot):
+        at = slot * block
         lat = keys_ref[j, :, :own, :].reshape(block, KV_RANK)
         packed = keys_ref[j, :, own:, :]
-        rope = jnp.concatenate(
+        key_cat[at : at + block, :KV_RANK] = lat
+        key_cat[at : at + block, KV_RANK : KV_RANK + ROPE] = jnp.concatenate(
             [packed[:, :, g * ROPE : (g + 1) * ROPE] for g in range(4)], axis=1
         ).reshape(block, ROPE)
-        key_cat[:, :KV_RANK] = lat
-        key_cat[:, KV_RANK : KV_RANK + ROPE] = rope
-        key_t[...] = lat.T
-        for h in range(heads_mla):
-            scores = dot_nt(key_cat[...], queries[h]) * scale
+        key_t[:, at : at + block] = lat.T
+
+    def attend(rows, ahead, late, diagonal=False):
+        chunks = [slice(at, at + width) for at in range(0, columns, width)]
+        ready, held = {}, []
+
+        def score(i):
+            ready[i] = dot_f32(key_cat[:rows, :], queries[:, chunks[i]])
+
+        def gather():
+            span, raw, rescale = held.pop(0)
+            acc[:, span] = acc[:, span] * rescale + dot_f32(key_t[:, :rows], raw)
+
+        for i in range(ahead):
+            score(i)
+        for i, span in enumerate(chunks):
+            if i + ahead < len(chunks):
+                score(i + ahead)
+            scores = ready.pop(i)
             if diagonal:
                 key_at = lax.broadcasted_iota(jnp.int32, scores.shape, 0)
-                query_at = lax.broadcasted_iota(jnp.int32, scores.shape, 1)
+                query_at = lax.broadcasted_iota(jnp.int32, scores.shape, 1) + span.start
+                query_at = lax.rem(query_at, block)
                 scores = jnp.where(key_at <= query_at, scores, MASKED_VALUE)
-            old = top[h]
-            new = jnp.maximum(old, jnp.max(scores, axis=0, keepdims=True))
-            raw = jnp.exp2(scores - new)
+            old = top[:, span]
+            new = jnp.maximum(old, jnp.max(scores, axis=0, keepdims=True) * scale)
+            raw = jnp.exp2(scores * scale - new)
             rescale = jnp.exp2(old - new)
-            total[h] = total[h] * rescale + jnp.sum(raw, axis=0, keepdims=True)
-            acc[h] = acc[h] * rescale + dot_f32(key_t[...], raw.astype(jnp.bfloat16))
-            top[h] = new
-
+            total[:, span] = total[:, span] * rescale + jnp.sum(raw, axis=0, keepdims=True)
+            top[:, span] = new
+            held.append((span, raw.astype(jnp.bfloat16), rescale))
+            if len(held) > late:
+                gather()
+        while held:
+            gather()
+
+    def received(n):
+        j, _ = block_at(n)
+        sends.pair(key(j), ktsend.at[j], ktrecv.at[j]).wait_recv()
+        return j
+
+    raise_own(3)
     with phase("w_lift1"):
         lift(1)
         fetch(jnp.int32(1))
     with phase("w_own"):
-        sends.pair(key(me), ktsend.at[me], ktrecv.at[me]).wait_recv()
+        received(jnp.int32(0))
     with phase("diag"):
-        update(me, True)
-
-    def step(n):
-        j, _ = block_at(n)
+        unpack(me, 0)
+        attend(block, 2, 0, True)
+
+    odd = lax.rem(me, 2)
+    with phase("w_two"):
+        fetch(jnp.int32(2))
+
+    @pl.when(odd == 1)
+    def _():
+        with phase("w_one"):
+            fetch(jnp.int32(3))
+            j = received(jnp.int32(1))
+        with phase("single"):
+            unpack(j, 0)
+            attend(block, 2, 0)
+
+    def two(p):
+        n = 1 + odd + 2 * p
         with phase("w_fetch"):
-            fetch(n + 1)
+            fetch(n + 2)
+            fetch(n + 3)
         with phase("w_pair"):
-            sends.pair(key(j), ktsend.at[j], ktrecv.at[j]).wait_recv()
-        with phase("update"):
-            update(j, False)
-
-    with phase("loop1"):
-        step_end = jnp.minimum(me + 1, 2)
-
-        @pl.loop(1, step_end)
-        def _(n):
-            step(n)
-
-    with phase("w_lift2"):
-        lift(2)
-    with phase("loop2"):
-
-        @pl.loop(2, jnp.minimum(me + 1, 3))
-        def _(n):
-            step(n)
-
-    with phase("w_lift3"):
-        lift(3)
-    with phase("loop3"):
-
-        @pl.loop(3, me + 1)
-        def _(n):
-            step(n)
+            j, jj = received(n), received(n + 1)
+        with phase("pair"):
+            unpack(j, 0)
+            unpack(jj, 1)
+            attend(2 * block, 1, 1)
+
+    pairs = lax.div(me, 2)
+
+    @pl.loop(0, pairs)
+    def _(p):
+        for d in (2, 3):
+
+            @pl.when(p == d - 1)
+            def _():
+                with phase("w_lift"):
+                    lift(d)
+
+        two(p)
 
     with phase("value_up"):
+        for copy in out_loads:
+            copy.wait()
         for h in range(heads_mla):
-            latent_out = (acc[h] / total[h]).astype(jnp.bfloat16)
+            span = slice(h * block, (h + 1) * block)
+            latent_out = (acc[:, span] / total[:, span]).astype(jnp.bfloat16)
             up = value_up_ref[:, pl.ds(pl.multiple_of((core * heads_mla + h) * VDIM, VDIM), VDIM)]
             mla_all[core, :, h * VDIM : (h + 1) * VDIM] = lax.dot_general(
                 latent_out, up, (((0,), (0,)), ((), ())), preferred_element_type=jnp.float32
@@ -718,8 +812,6 @@
     mla_swap = swap_all(mla_all, 3)
     with phase("w_finish"):
         swa_swap.wait_recv()
-        for load in out_loads:
-            load.wait()
     width_out = heads_mla * VDIM
 
     def product(values, first):
@@ -739,6 +831,15 @@
         out_ref[...] = mixed.astype(jnp.bfloat16)
     sends.finish()
     pl.when(has_next)(lambda: edge.wait_send())
+    for copy, cond in zip(beside_keys(me, 0), own_conds):
+        pl.when(cond)(lambda copy=copy: copy.wait_send())
+    for d in range(1, PLANES):
+
+        @pl.when(z >= d)
+        def _():
+            for copy in beside_keys((z - d) * PLANE + c, d):
+                copy.wait_send()
+
 
     @pl.loop(0, me + 1)
     def _(j):
@@ -768,9 +869,11 @@
     width_mla, width_swa, width_kv = mla_query.shape[1], swa_query.shape[1], swa_key.shape[1]
     heads_mla = width_mla // (NOPE + ROPE)
     width_all = width_mla + width_swa + 2 * width_kv
-    inverse = ROPE_BASE ** (-jnp.arange(0, ROPE, 2, dtype=jnp.float32) / ROPE)
-    positions = lax.axis_index("sp") * block + jnp.arange(block, dtype=jnp.int32)
-    angles = positions.astype(jnp.float32)[:, None] * inverse[None, :]
+    inverse = ROPE_BASE ** (-np.arange(0, ROPE, 2, dtype=np.float64) / ROPE)
+    near = np.arange(block)[:, None] * inverse
+    far = (np.arange(count) * block)[:, None] * inverse
+    turns = np.concatenate([np.cos(near), np.sin(near)], axis=1).astype(np.float32)
+    bases = np.concatenate([np.cos(far), np.sin(far)], axis=1).astype(np.float32)
     down_rows = latent_down.shape[0]
     shard_rows = down_rows // 2 + down_rows // 2 * ROPE // KV_RANK
     key_rows = own + own * ROPE // KV_RANK
@@ -780,20 +883,28 @@
     return pl.pallas_call(
         lambda *refs: layer_kernel(count, *refs),
         out_shape=jax.ShapeDtypeStruct((block, out_mla.shape[1]), bf16),
-        in_specs=[vmem] * 8
-        + [pl.BlockSpec(memory_space=pltpu.SMEM)]
-        + [hbm] * 4
-        + [vmem]
-        + [hbm] * 2,
+        in_specs=[hbm] * 16,
         out_specs=vmem,
         scratch_shapes=[
+            pltpu.VMEM((own, depth), bf16),
+            pltpu.VMEM((1, depth), jnp.float32),
+            pltpu.VMEM((ROPE, down_rows), bf16),
+            pltpu.VMEM((1, KV_RANK), jnp.float32),
+            pltpu.VMEM((block, ROPE), jnp.float32),
+            pltpu.VMEM((1, ROPE), jnp.float32),
+            pltpu.VMEM(key_up.shape, bf16),
+            pltpu.SMEM(sink_logits.shape, jnp.float32),
+            pltpu.VMEM(value_up.shape, bf16),
+            pltpu.VMEM((block, ROPE // 2), jnp.float32),
+            pltpu.VMEM((block, ROPE // 2), jnp.float32),
+            pltpu.VMEM((ROPE, depth), bf16),
             pltpu.VMEM((count, cores, key_rows, KV_RANK), bf16),
-            pltpu.VMEM((heads_mla, block, KV_RANK + 2 * ROPE), bf16),
-            pltpu.VMEM((block, KV_RANK + 2 * ROPE), bf16),
-            pltpu.VMEM((KV_RANK, block), bf16),
-            pltpu.VMEM((heads_mla, 1, block), jnp.float32),
-            pltpu.VMEM((heads_mla, 1, block), jnp.float32),
-            pltpu.VMEM((heads_mla, KV_RANK, block), jnp.float32),
+            pltpu.VMEM((KV_RANK + 2 * ROPE, heads_mla * block), bf16),
+            pltpu.VMEM((2 * block, KV_RANK + 2 * ROPE), bf16),
+            pltpu.VMEM((KV_RANK, 2 * block), bf16),
+            pltpu.VMEM((1, heads_mla * block), jnp.float32),
+            pltpu.VMEM((1, heads_mla * block), jnp.float32),
+            pltpu.VMEM((KV_RANK, heads_mla * block), jnp.float32),
             pltpu.VMEM((cores, block, heads_mla * VDIM), bf16),
             pltpu.VMEM((cores, block, width_swa), bf16),
             pltpu.VMEM((out_mla.shape[0] + out_swa.shape[0], out_mla.shape[1]), bf16),
@@ -802,7 +913,7 @@
             pltpu.VMEM((block, width_all), bf16),
             pltpu.VMEM((count, cores, shard_rows, KV_RANK), bf16),
             pltpu.VMEM((WINDOW + block, 2 * width_kv), bf16),
-            pltpu.SemaphoreType.DMA((6,)),
+            pltpu.SemaphoreType.DMA((16,)),
             pltpu.SemaphoreType.DMA((6 + 3 * PLANES,)),
             pltpu.SemaphoreType.DMA((count,)),
             pltpu.SemaphoreType.DMA((PLANES,)),
@@ -822,10 +933,10 @@
         inputs,
         norm_gain[None, :],
         latent_down,
-        rope_down,
+        rope_down.T,
         latent_gain[None, :],
-        jnp.cos(angles),
-        jnp.sin(angles),
+        turns,
+        bases[:, None, :],
         key_up,
         sink_logits,
         mla_query,

time: 73.2 us -> 59.6 us (0.81)
  the two profiles are of different devices: /device:TPU:31 before, /device:TPU:27 now
where the time goes in v2:
time: 59.6 us; the launch traced here: 59.4 us
  Pallas kernels  57.3 us (96%)
  local copies, waits for them, and re-layouts  2.06 us (3%)
    pallas_call x1, Pallas kernels, fast_shards(): pl.pallas_call(lambda *refs: layer_kernel(count, *refs), out_shape=jax.Sh...  57.3 us
    unnamed x1, local copies, waits for them, and re-layouts  2.06 us

profile of v2, /device:TPU:27, one launch (start us, length us, event | category | flops | bytes accessed | tf_op | source)
XLA Modules:
  0.0 59.4 jit_solution(2119171656762990473)
XLA Ops:
  0.0 57.3 %layer.1 = bf16[384,1024]{1,0:T(8,128)(2,1)} custom-call(bf16[192,2048]{1,0:T(8,128)(2,1)} %refs_0_.1, f32[1,2048]{1,0:T(1,128)} %bitcast.4, bf16[128,256]{1,0:T(8,128)(2,1)} %refs_2_.1, bf16[64,128]{1,0:T(8,128)(2,1)} %bitcast.3, f32[1,256]{1,0:T(1,128)} %bitcast.5, f32[384,64]{1,0:T(8,128)} %constant.4.clone.refs_5_, f32[16,1,64]{2,1,0:T(1,128)} %constant.5.clone.refs_6_, ...), custom_call_target="tpu_custom_call" | custom-call | tf_op jit(solution)/shard_map/layer/pallas_call | solution.py:883
  57.4 2.1 %copy.18 = bf16[384,1024]{1,0:T(8,128)(2,1)} copy(bf16[384,1024]{1,0:T(8,128)(2,1)} %layer.1) | data formatting | bytes 1572864

commit v3 on v2

--- a/solution.py
+++ b/solution.py
@@ -449,7 +449,7 @@
     out_loads = [load(value_up_hbm, value_up_ref)]
     for i, ref in enumerate((out_mla_ref, out_swa_ref)):
         out_loads.append(load(ref, out_weights.at[pl.ds(i * out_rows, out_rows)]))
-    for copy in early + loads + small:
+    for copy in early + loads[2:] + loads[:2] + small:
         copy.start()
 
     with phase("w_first"):
@@ -505,36 +505,7 @@
     swap = sends.go(
         normed.at[pl.ds(mine, own)], {"tp": 1 - core}, xsend.at[0], xrecv.at[0]
     )
-    with phase("w_loads"):
-        for copy in loads:
-            copy.wait()
-
-    for copy in out_loads:
-        copy.start()
-
-    def project(at):
-        lhs = normed[pl.ds(at, own), :]
-        for j in range(0, proj.shape[1], 256):
-            proj[pl.ds(at, own), j : j + 256] = dot_f32(lhs, weights[:, j : j + 256]).astype(
-                jnp.bfloat16
-            )
-
-    def arrived(part, recv):
-        sends.pair(part, xsend.at[0], recv).wait_recv()
-
-    with phase("proj1"):
-        project(mine)
-    for level, zz in enumerate(others):
-        with phase("w_z"):
-            arrived(shard(zz * PLANE + c), wrecv.at[zz * PLANE + c])
-        spread(zz * PLANE + c, level + 1)
-    with phase("w_swap"):
-        swap.wait_recv()
-    with phase("proj2"):
-        project(other)
-
     kv = width_mla + width_swa
-    window[WINDOW:, :] = proj[:, kv:]
     has_next, has_last = me < count - 1, me > 0
     edge_rows = window.at[pl.ds(block, WINDOW)]
     edge = pltpu.make_async_remote_copy(
@@ -546,9 +517,50 @@
         device_id_type=MESH,
     )
 
-    @pl.when(has_next)
-    def _():
-        edge.start()
+    def project_edge():
+        lhs = normed[block - WINDOW :, :]
+        for j in range(0, 2 * width_kv, 256):
+            window[block:, j : j + 256] = dot_f32(
+                lhs, weights[:, kv + j : kv + j + 256]
+            ).astype(jnp.bfloat16)
+        pl.when(has_next)(lambda: edge.start())
+
+    with phase("w_loads2"):
+        for copy in loads[2:]:
+            copy.wait()
+    with phase("edge1"):
+        pl.when(core == 1)(project_edge)
+    with phase("w_loads"):
+        for copy in loads[:2]:
+            copy.wait()
+
+    for copy in out_loads:
+        copy.start()
+
+    def project(at):
+        lhs = normed[pl.ds(at, own), :]
+        for j in range(0, proj.shape[1], 256):
+            proj[pl.ds(at, own), j : j + 256] = dot_f32(lhs, weights[:, j : j + 256]).astype(
+                jnp.bfloat16
+            )
+
+    def arrived(part, recv):
+        sends.pair(part, xsend.at[0], recv).wait_recv()
+
+    with phase("proj1"):
+        project(mine)
+    with phase("w_swap"):
+        swap.wait_recv()
+    with phase("edge0"):
+        pl.when(core == 0)(project_edge)
+    for level, zz in enumerate(others):
+        with phase("w_z"):
+            arrived(shard(zz * PLANE + c), wrecv.at[zz * PLANE + c])
+        spread(zz * PLANE + c, level + 1)
+    with phase("proj2"):
+        project(other)
+
+    window[WINDOW:block, :] = proj[: block - WINDOW, kv:]
 
     @pl.when(me == 0)
     def _():
@@ -582,9 +594,6 @@
             queries[KV_RANK : KV_RANK + ROPE, span] = turn(
                 proj[:, base + NOPE : base + NOPE + ROPE], cos, sin
             ).T
-    for level, zz in enumerate(others):
-        handed.append(hand_over(zz, level + 1))
-
     row = lax.broadcasted_iota(jnp.int32, (WINDOW, 2 * WINDOW), 0)
     column_of = lax.broadcasted_iota(jnp.int32, (WINDOW, 2 * WINDOW), 1)
     distance = row + WINDOW - column_of
@@ -609,6 +618,12 @@
             outs.append(dot_f32((raw / total).astype(jnp.bfloat16), v).astype(jnp.bfloat16))
         swa_all[core, at : at + WINDOW, :] = jnp.concatenate(outs, axis=1)
 
+    with phase("w_edge"):
+        pl.when(has_last)(lambda: edge.wait_recv())
+    with phase("win0"):
+        windowed(0)
+    for level, zz in enumerate(others):
+        handed.append(hand_over(zz, level + 1))
     with phase("w_handed"):
         for copy in handed:
             copy.wait_recv()
@@ -637,16 +652,15 @@
     def key(j):
         return keys_ref.at[pl.ds(j, 1), pl.ds(core, 1)]
 
-    def raise_own(d):
-        sends.go(
-            key(me), {"sp": me + d * PLANE}, ksend.at[d - 1], krecv.at[me], z + d < PLANES
-        )
-
-    raise_own(1)
+    def raised(j, d):
+        return sends.copy(key(j), {"sp": me + PLANE}, ksend.at[d], krecv.at[j])
+
+    inner = z + 1 < PLANES
+    pl.when(inner)(lambda: raised(me, 0).start())
 
     def beside_keys(j, level):
         return [
-            sends.copy(key(j), {"sp": beside[q]}, ksend.at[3 + 3 * level + q], krecv.at[j])
+            sends.copy(key(j), {"sp": beside[q]}, ksend.at[PLANES + 3 * level + q], krecv.at[j])
             for q in range(PLANE - 1)
         ]
 
@@ -662,15 +676,24 @@
         later = jnp.maximum(n - c - 1, 0)
         q = lax.rem(later, PLANE)
         j = (z - lax.div(later, PLANE) - 1) * PLANE + column(q)
-        first = jnp.logical_and(n > c, q == 0)
-        return jnp.where(n <= c, me - n, j), first
+        q = jnp.where(n <= c, PLANE, q)
+        return jnp.where(n <= c, me - n, j), q, lax.div(later, PLANE) + 1
+
+    def climb(j, level):
+        slot = PLANES + 3 * (level + 1) + 2
+        return sends.copy(key(j), {"sp": me + PLANE}, ksend.at[slot], krecv.at[j])
 
     def fetch(n):
-        j, first = block_at(n)
-
-        @pl.when(jnp.logical_and(n <= me, jnp.logical_not(first)))
+        j, q, level = block_at(n)
+
+        @pl.when(jnp.logical_and(n <= me, q > 0))
         def _():
             arrived(key(j), krecv.at[j])
+
+            @pl.when(jnp.logical_and(q == PLANE - 1, inner))
+            def _():
+                climb(j, level).start()
+
             pass_on(j)
 
     def lift(d):
@@ -678,7 +701,8 @@
         def _():
             j = (z - d) * PLANE + c
             arrived(key(j), krecv.at[j])
-            for copy in beside_keys(j, d):
+            pl.when(inner)(lambda: raised(j, d).start())
+            for copy in beside_keys(j, d)[: 3 if d == 1 else 2]:
                 copy.start()
             pass_on(j)
 
@@ -690,11 +714,7 @@
     with phase("win12"):
         for tile in range(1, block // WINDOW):
             windowed(tile)
-    raise_own(2)
-    with phase("w_edge"):
-        pl.when(has_last)(lambda: edge.wait_recv())
-    with phase("win0"):
-        windowed(0)
+
     swa_swap = swap_all(swa_all, 2)
 
     top[...] = jnp.full_like(top, MASKED_VALUE)
@@ -747,19 +767,19 @@
             gather()
 
     def received(n):
-        j, _ = block_at(n)
+        j = block_at(n)[0]
         sends.pair(key(j), ktsend.at[j], ktrecv.at[j]).wait_recv()
         return j
 
-    raise_own(3)
-    with phase("w_lift1"):
-        lift(1)
-        fetch(jnp.int32(1))
     with phase("w_own"):
         received(jnp.int32(0))
     with phase("diag"):
         unpack(me, 0)
         attend(block, 2, 0, True)
+    with phase("w_lift1"):
+        lift(1)
+    with phase("w_fetch1"):
+        fetch(jnp.int32(1))
 
     odd = lax.rem(me, 2)
     with phase("w_two"):
@@ -790,9 +810,9 @@
 
     @pl.loop(0, pairs)
     def _(p):
-        for d in (2, 3):
-
-            @pl.when(p == d - 1)
+        for d, turn_at in ((2, cy), (3, cy + 2)):
+
+            @pl.when(p == turn_at)
             def _():
                 with phase("w_lift"):
                     lift(d)
@@ -833,12 +853,18 @@
     pl.when(has_next)(lambda: edge.wait_send())
     for copy, cond in zip(beside_keys(me, 0), own_conds):
         pl.when(cond)(lambda copy=copy: copy.wait_send())
+    pl.when(inner)(lambda: raised(me, 0).wait_send())
     for d in range(1, PLANES):
 
         @pl.when(z >= d)
         def _():
-            for copy in beside_keys((z - d) * PLANE + c, d):
+            j = (z - d) * PLANE + c
+            pl.when(inner)(lambda: raised(j, d).wait_send())
+            for copy in beside_keys(j, d)[: 3 if d == 1 else 2]:
                 copy.wait_send()
+            if d < PLANES - 1:
+                far = (z - d) * PLANE + PLANE - 1 - c
+                pl.when(inner)(lambda: climb(far, d).wait_send())
 
 
     @pl.loop(0, me + 1)
@@ -918,7 +944,7 @@
             pltpu.SemaphoreType.DMA((count,)),
             pltpu.SemaphoreType.DMA((PLANES,)),
             pltpu.SemaphoreType.DMA((PLANES,)),
-            pltpu.SemaphoreType.DMA((3 + 3 * PLANES,)),
+            pltpu.SemaphoreType.DMA((4 * PLANES,)),
             pltpu.SemaphoreType.DMA((count,)),
             pltpu.SemaphoreType.DMA((count,)),
             pltpu.SemaphoreType.DMA((count,)),

time: 59.6 us -> 54.9 us (0.921)
  Pallas kernels: 57.3 us -> 52.5 us
    pallas_call x1, Pallas kernels: 57.3 us -> 52.5 us  [fast_shards(): pl.pallas_call(lambda *refs: layer_kernel(count, *refs), out_shape=jax.Sh...]
where the time goes in v3:
time: 54.9 us; the launch traced here: 54.6 us
  Pallas kernels  52.5 us (96%)
  local copies, waits for them, and re-layouts  2.06 us (4%)
    pallas_call x1, Pallas kernels, fast_shards(): pl.pallas_call(lambda *refs: layer_kernel(count, *refs), out_shape=jax.Sh...  52.5 us
    unnamed x1, local copies, waits for them, and re-layouts  2.06 us

profile of v3, /device:TPU:27, one launch (start us, length us, event | category | flops | bytes accessed | tf_op | source)
XLA Modules:
  0.0 54.6 jit_solution(5942666089023202468)
XLA Ops:
  0.0 52.5 %layer.1 = bf16[384,1024]{1,0:T(8,128)(2,1)} custom-call(bf16[192,2048]{1,0:T(8,128)(2,1)} %refs_0_.1, f32[1,2048]{1,0:T(1,128)} %bitcast.4, bf16[128,256]{1,0:T(8,128)(2,1)} %refs_2_.1, bf16[64,128]{1,0:T(8,128)(2,1)} %bitcast.3, f32[1,256]{1,0:T(1,128)} %bitcast.5, f32[384,64]{1,0:T(8,128)} %constant.4.clone.refs_5_, f32[16,1,64]{2,1,0:T(1,128)} %constant.5.clone.refs_6_, ...), custom_call_target="tpu_custom_call" | custom-call | tf_op jit(solution)/shard_map/layer/pallas_call | solution.py:909
  52.5 2.1 %copy.18 = bf16[384,1024]{1,0:T(8,128)(2,1)} copy(bf16[384,1024]{1,0:T(8,128)(2,1)} %layer.1) | data formatting | bytes 1572864

commit v4 on v3

--- a/solution.py
+++ b/solution.py
@@ -449,7 +449,7 @@
     out_loads = [load(value_up_hbm, value_up_ref)]
     for i, ref in enumerate((out_mla_ref, out_swa_ref)):
         out_loads.append(load(ref, out_weights.at[pl.ds(i * out_rows, out_rows)]))
-    for copy in early + loads[2:] + loads[:2] + small:
+    for copy in early + loads[2:] + loads[1::-1] + small:
         copy.start()
 
     with phase("w_first"):
@@ -467,19 +467,22 @@
     def shard(j):
         return gathered.at[pl.ds(j, 1), pl.ds(core, 1)]
 
-    for d in range(PLANES - 1, 0, -1):
-        for k, step in enumerate((d, -d)):
-            cond = (z + step < PLANES) if step > 0 else (z + step >= 0)
-            sends.go(
-                shard(me),
-                {"sp": me + step * PLANE},
-                wsend.at[2 * (d - 1) + k],
-                wrecv.at[me],
-                cond,
-            )
+    def along(j, first):
+        for d in range(PLANES - 1, 0, -1):
+            for k, step in enumerate((d, -d)):
+                cond = (z + step < PLANES) if step > 0 else (z + step >= 0)
+                sends.go(
+                    shard(j),
+                    {"sp": me + step * PLANE},
+                    wsend.at[first + 2 * (d - 1) + k],
+                    wrecv.at[j],
+                    cond,
+                )
+
+    along(me, 0)
 
     def spread(j, level):
-        for q in range(PLANE - 1):
+        for q in range(PLANE - 1 if level == 0 else 2):
             sends.go(
                 shard(j), {"sp": beside[q]}, wsend.at[6 + 3 * level + q], wrecv.at[j]
             )
@@ -530,16 +533,9 @@
             copy.wait()
     with phase("edge1"):
         pl.when(core == 1)(project_edge)
-    with phase("w_loads"):
-        for copy in loads[:2]:
-            copy.wait()
-
-    for copy in out_loads:
-        copy.start()
-
-    def project(at):
+    def project(at, low, high):
         lhs = normed[pl.ds(at, own), :]
-        for j in range(0, proj.shape[1], 256):
+        for j in range(low, high, 256):
             proj[pl.ds(at, own), j : j + 256] = dot_f32(lhs, weights[:, j : j + 256]).astype(
                 jnp.bfloat16
             )
@@ -548,17 +544,31 @@
         sends.pair(part, xsend.at[0], recv).wait_recv()
 
     with phase("proj1"):
-        project(mine)
+        project(mine, kv, proj.shape[1])
+    with phase("w_loads"):
+        loads[1].wait()
+    with phase("proj1"):
+        project(mine, width_mla, kv)
+    with phase("w_loads"):
+        loads[0].wait()
+    for copy in out_loads:
+        copy.start()
+    with phase("proj1"):
+        project(mine, 0, width_mla)
     with phase("w_swap"):
         swap.wait_recv()
     with phase("edge0"):
         pl.when(core == 0)(project_edge)
+    with phase("w_diag"):
+        across = beside[PLANE - 2]
+        arrived(shard(across), wrecv.at[across])
+    along(across, 6 + 3 * PLANES)
     for level, zz in enumerate(others):
         with phase("w_z"):
             arrived(shard(zz * PLANE + c), wrecv.at[zz * PLANE + c])
         spread(zz * PLANE + c, level + 1)
     with phase("proj2"):
-        project(other)
+        project(other, 0, proj.shape[1])
 
     window[WINDOW:block, :] = proj[: block - WINDOW, kv:]
 
@@ -568,7 +578,7 @@
 
     def hand_over(zz, level):
         with phase("w_plane"):
-            for q in range(1, PLANE):
+            for q in range(1, PLANE if level else PLANE - 1):
                 j = zz * PLANE + column(jnp.int32(q))
                 arrived(shard(j), wrecv.at[j])
         part = gathered.at[pl.ds(zz * PLANE, PLANE), pl.ds(core, 1)]
@@ -618,10 +628,8 @@
             outs.append(dot_f32((raw / total).astype(jnp.bfloat16), v).astype(jnp.bfloat16))
         swa_all[core, at : at + WINDOW, :] = jnp.concatenate(outs, axis=1)
 
-    with phase("w_edge"):
-        pl.when(has_last)(lambda: edge.wait_recv())
-    with phase("win0"):
-        windowed(0)
+    with phase("win1"):
+        windowed(1)
     for level, zz in enumerate(others):
         handed.append(hand_over(zz, level + 1))
     with phase("w_handed"):
@@ -673,11 +681,21 @@
     pass_on(me)
 
     def block_at(n):
-        later = jnp.maximum(n - c - 1, 0)
-        q = lax.rem(later, PLANE)
-        j = (z - lax.div(later, PLANE) - 1) * PLANE + column(q)
-        q = jnp.where(n <= c, PLANE, q)
-        return jnp.where(n <= c, me - n, j), q, lax.div(later, PLANE) + 1
+        late = jnp.where(n > 1, 1, 0)
+        latest = jnp.where(n > 2, 1, 0)
+        i = jnp.where(
+            cy == 0,
+            jnp.where(cx == 0, n + 1 + late, n - 1 + late + latest),
+            jnp.where(cx == 0, n, n - 1),
+        )
+
+        def exchanged(at):
+            return jnp.where(i == at, 1, 0) - jnp.where(i == at + 1, 1, 0)
+
+        v = i + 1 + jnp.where(z > 0, exchanged(2), 0) + jnp.where(z > 1, exchanged(6), 0)
+        v = jnp.where(n == 0, 0, v)
+        level, q = lax.div(v, PLANE), lax.rem(v, PLANE)
+        return (z - level) * PLANE + column(q), q, level
 
     def climb(j, level):
         slot = PLANES + 3 * (level + 1) + 2
@@ -690,7 +708,7 @@
         def _():
             arrived(key(j), krecv.at[j])
 
-            @pl.when(jnp.logical_and(q == PLANE - 1, inner))
+            @pl.when(jnp.logical_and(jnp.logical_and(q == PLANE - 1, level > 0), inner))
             def _():
                 climb(j, level).start()
 
@@ -712,10 +730,9 @@
         )
 
     with phase("win12"):
-        for tile in range(1, block // WINDOW):
+        for tile in range(2, block // WINDOW):
             windowed(tile)
 
-    swa_swap = swap_all(swa_all, 2)
 
     top[...] = jnp.full_like(top, MASKED_VALUE)
     total[...] = jnp.zeros_like(total)
@@ -732,7 +749,7 @@
         ).reshape(block, ROPE)
         key_t[:, at : at + block] = lat.T
 
-    def attend(rows, ahead, late, diagonal=False):
+    def attend(rows, ahead, late, diagonal=False, hook=None):
         chunks = [slice(at, at + width) for at in range(0, columns, width)]
         ready, held = {}, []
 
@@ -763,8 +780,16 @@
             held.append((span, raw.astype(jnp.bfloat16), rescale))
             if len(held) > late:
                 gather()
+            if hook is not None and i == len(chunks) - 2:
+                hook()
         while held:
             gather()
+
+    width_out = heads_mla * VDIM
+
+    def product(values, first):
+        rows = values.shape[1]
+        return dot_f32(values, out_weights[pl.ds(pl.multiple_of(first, rows), rows), :])
 
     def received(n):
         j = block_at(n)[0]
@@ -773,34 +798,56 @@
 
     with phase("w_own"):
         received(jnp.int32(0))
+    odd = lax.rem(me, 2)
     with phase("diag"):
         unpack(me, 0)
         attend(block, 2, 0, True)
+    with phase("w_edge"):
+        pl.when(has_last)(lambda: edge.wait_recv())
+    with phase("win0"):
+        windowed(0)
+    swa_swap = swap_all(swa_all, 2)
     with phase("w_lift1"):
         lift(1)
     with phase("w_fetch1"):
         fetch(jnp.int32(1))
 
-    odd = lax.rem(me, 2)
-    with phase("w_two"):
-        fetch(jnp.int32(2))
+    @pl.when(odd == 0)
+    def _():
+        with phase("w_two"):
+            fetch(jnp.int32(2))
 
     @pl.when(odd == 1)
     def _():
         with phase("w_one"):
-            fetch(jnp.int32(3))
             j = received(jnp.int32(1))
+
+        def onward():
+            with phase("w_fetch"):
+                fetch(jnp.int32(2))
+                fetch(jnp.int32(3))
+
         with phase("single"):
             unpack(j, 0)
             attend(block, 2, 0)
+        onward()
 
     def two(p):
         n = 1 + odd + 2 * p
-        with phase("w_fetch"):
-            fetch(n + 2)
-            fetch(n + 3)
         with phase("w_pair"):
             j, jj = received(n), received(n + 1)
+
+        def onward():
+            @pl.when(p == cy + 1)
+            def _():
+                with phase("w_lift3"):
+                    lift(3)
+
+            with phase("w_fetch"):
+                fetch(n + 2)
+                fetch(n + 3)
+
+        onward()
         with phase("pair"):
             unpack(j, 0)
             unpack(jj, 1)
@@ -810,12 +857,10 @@
 
     @pl.loop(0, pairs)
     def _(p):
-        for d, turn_at in ((2, cy), (3, cy + 2)):
-
-            @pl.when(p == turn_at)
-            def _():
-                with phase("w_lift"):
-                    lift(d)
+        @pl.when(p == cy)
+        def _():
+            with phase("w_lift2"):
+                lift(2)
 
         two(p)
 
@@ -830,15 +875,8 @@
                 latent_out, up, (((0,), (0,)), ((), ())), preferred_element_type=jnp.float32
             ).astype(jnp.bfloat16)
     mla_swap = swap_all(mla_all, 3)
-    with phase("w_finish"):
+    with phase("out1"):
         swa_swap.wait_recv()
-    width_out = heads_mla * VDIM
-
-    def product(values, first):
-        width = values.shape[1]
-        return dot_f32(values, out_weights[pl.ds(pl.multiple_of(first, width), width), :])
-
-    with phase("out1"):
         own_part = (
             product(swa_all[0], out_rows)
             + product(swa_all[1], out_rows + width_swa)
@@ -940,7 +978,7 @@
             pltpu.VMEM((count, cores, shard_rows, KV_RANK), bf16),
             pltpu.VMEM((WINDOW + block, 2 * width_kv), bf16),
             pltpu.SemaphoreType.DMA((16,)),
-            pltpu.SemaphoreType.DMA((6 + 3 * PLANES,)),
+            pltpu.SemaphoreType.DMA((12 + 3 * PLANES,)),
             pltpu.SemaphoreType.DMA((count,)),
             pltpu.SemaphoreType.DMA((PLANES,)),
             pltpu.SemaphoreType.DMA((PLANES,)),

time: 54.9 us -> 52.9 us (0.964); the launches traced: 54.6 us -> 52 us
  Pallas kernels: 52.5 us -> 49.9 us
    pallas_call x1, Pallas kernels: 52.5 us -> 49.9 us  [fast_shards(): pl.pallas_call(lambda *refs: layer_kernel(count, *refs), out_shape=jax.Sh...]
where the time goes in v4:
time: 52.9 us; the launch traced here: 52 us
  Pallas kernels  49.9 us (94%)
  local copies, waits for them, and re-layouts  2.06 us (4%)
    pallas_call x1, Pallas kernels, fast_shards(): pl.pallas_call(lambda *refs: layer_kernel(count, *refs), out_shape=jax.Sh...  49.9 us
    unnamed x1, local copies, waits for them, and re-layouts  2.06 us

profile of v4, /device:TPU:27, one launch (start us, length us, event | category | flops | bytes accessed | tf_op | source)
XLA Modules:
  0.0 52.0 jit_solution(13502991073305229912)
XLA Ops:
  0.0 49.9 %layer.1 = bf16[384,1024]{1,0:T(8,128)(2,1)} custom-call(bf16[192,2048]{1,0:T(8,128)(2,1)} %refs_0_.1, f32[1,2048]{1,0:T(1,128)} %bitcast.4, bf16[128,256]{1,0:T(8,128)(2,1)} %refs_2_.1, bf16[64,128]{1,0:T(8,128)(2,1)} %bitcast.3, f32[1,256]{1,0:T(1,128)} %bitcast.5, f32[384,64]{1,0:T(8,128)} %constant.4.clone.refs_5_, f32[16,1,64]{2,1,0:T(1,128)} %constant.5.clone.refs_6_, ...), custom_call_target="tpu_custom_call" | custom-call | tf_op jit(solution)/shard_map/layer/pallas_call | solution.py:947
  49.9 2.1 %copy.18 = bf16[384,1024]{1,0:T(8,128)(2,1)} copy(bf16[384,1024]{1,0:T(8,128)(2,1)} %layer.1) | data formatting | bytes 1572864

commit v5 on v4

--- a/solution.py
+++ b/solution.py
@@ -588,8 +588,6 @@
     with phase("queries"):
         for copy in small:
             copy.wait()
-        key_cat[...] = jnp.zeros_like(key_cat)
-        queries[KV_RANK + ROPE :, :] = jnp.zeros_like(queries[KV_RANK + ROPE :, :])
         half = ROPE // 2
         base_cos, base_sin = base_ref[:, :half], base_ref[:, half:]
         near_cos, near_sin = turns_ref[:, :half], turns_ref[:, half:]
@@ -620,12 +618,13 @@
             q = proj[at : at + WINDOW, width_mla + h * HEAD : width_mla + (h + 1) * HEAD]
             k = window[at : at + 2 * WINDOW, g * HEAD : (g + 1) * HEAD]
             v = window[at : at + 2 * WINDOW, width_kv + g * HEAD : width_kv + (g + 1) * HEAD]
-            scores = jnp.where(allowed, dot_nt(q, k) * HEAD ** (-0.5), MASKED_VALUE)
-            sink = jnp.zeros((WINDOW, 1), jnp.float32) + sink_ref[core * heads_swa + h]
+            scores = jnp.where(allowed, dot_nt(q, k) * (HEAD ** (-0.5) * LOG2E), MASKED_VALUE)
+            sink = jnp.zeros((WINDOW, 1), jnp.float32) + sink_ref[core * heads_swa + h] * LOG2E
             top = jnp.maximum(jnp.max(scores, axis=-1, keepdims=True), sink)
-            raw = jnp.exp(scores - top)
-            total = jnp.sum(raw, axis=-1, keepdims=True) + jnp.exp(sink - top)
-            outs.append(dot_f32((raw / total).astype(jnp.bfloat16), v).astype(jnp.bfloat16))
+            raw = jnp.exp2(scores - top)
+            total = jnp.sum(raw, axis=-1, keepdims=True) + jnp.exp2(sink - top)
+            share = (raw * (1.0 / total)).astype(jnp.bfloat16)
+            outs.append(dot_f32(share, v).astype(jnp.bfloat16))
         swa_all[core, at : at + WINDOW, :] = jnp.concatenate(outs, axis=1)
 
     with phase("win1"):
@@ -869,7 +868,7 @@
             copy.wait()
         for h in range(heads_mla):
             span = slice(h * block, (h + 1) * block)
-            latent_out = (acc[:, span] / total[:, span]).astype(jnp.bfloat16)
+            latent_out = (acc[:, span] * (1.0 / total[:, span])).astype(jnp.bfloat16)
             up = value_up_ref[:, pl.ds(pl.multiple_of((core * heads_mla + h) * VDIM, VDIM), VDIM)]
             mla_all[core, :, h * VDIM : (h + 1) * VDIM] = lax.dot_general(
                 latent_out, up, (((0,), (0,)), ((), ())), preferred_element_type=jnp.float32
@@ -946,7 +945,7 @@
     bf16 = jnp.bfloat16
     return pl.pallas_call(
         lambda *refs: layer_kernel(count, *refs),
-        out_shape=jax.ShapeDtypeStruct((block, out_mla.shape[1]), bf16),
+        out_shape=pltpu.VMEM((block, out_mla.shape[1]), bf16),
         in_specs=[hbm] * 16,
         out_specs=vmem,
         scratch_shapes=[
@@ -963,8 +962,8 @@
             pltpu.VMEM((block, ROPE // 2), jnp.float32),
             pltpu.VMEM((ROPE, depth), bf16),
             pltpu.VMEM((count, cores, key_rows, KV_RANK), bf16),
-            pltpu.VMEM((KV_RANK + 2 * ROPE, heads_mla * block), bf16),
-            pltpu.VMEM((2 * block, KV_RANK + 2 * ROPE), bf16),
+            pltpu.VMEM((KV_RANK + ROPE, heads_mla * block), bf16),
+            pltpu.VMEM((2 * block, KV_RANK + ROPE), bf16),
             pltpu.VMEM((KV_RANK, 2 * block), bf16),
             pltpu.VMEM((1, heads_mla * block), jnp.float32),
             pltpu.VMEM((1, heads_mla * block), jnp.float32),

time: 52.9 us -> 50.7 us (0.958)
  local copies, waits for them, and re-layouts: 2.06 us -> 0.88 us
  Pallas kernels: 49.9 us -> 48.9 us
    unnamed x1, local copies, waits for them, and re-layouts: 2.06 us -> 0.88 us
    pallas_call x1, Pallas kernels: 49.9 us -> 48.9 us  [fast_shards(): pl.pallas_call(lambda *refs: layer_kernel(count, *refs), out_shape=pltpu....]
where the time goes in v5:
time: 50.7 us; the launch traced here: 49.8 us
  Pallas kernels  48.9 us (96%)
  local copies, waits for them, and re-layouts  0.88 us (2%)
    pallas_call x1, Pallas kernels, fast_shards(): pl.pallas_call(lambda *refs: layer_kernel(count, *refs), out_shape=pltpu....  48.9 us

profile of v5, /device:TPU:27, one launch (start us, length us, event | category | flops | bytes accessed | tf_op | source)
XLA Modules:
  0.0 49.8 jit_solution(17049579409929100014)
XLA Ops:
  0.0 48.9 %layer.1 = bf16[384,1024]{1,0:T(8,128)(2,1)S(1)} custom-call(bf16[192,2048]{1,0:T(8,128)(2,1)} %refs_0_.1, f32[1,2048]{1,0:T(1,128)} %bitcast.4, bf16[128,256]{1,0:T(8,128)(2,1)} %refs_2_.1, bf16[64,128]{1,0:T(8,128)(2,1)} %bitcast.3, f32[1,256]{1,0:T(1,128)} %bitcast.5, f32[384,64]{1,0:T(8,128)} %constant.4.clone.refs_5_, ...), custom_call_target="tpu_custom_call" | custom-call | tf_op jit(solution)/shard_map/layer/pallas_call | solution.py:946
  48.9 0.9 %copy.18 = bf16[384,1024]{1,0:T(8,128)(2,1)} copy(bf16[384,1024]{1,0:T(8,128)(2,1)S(1)} %layer.1) | data formatting | bytes 1572864

commit v6 on v5

--- a/solution.py
+++ b/solution.py
@@ -806,10 +806,13 @@
     with phase("win0"):
         windowed(0)
     swa_swap = swap_all(swa_all, 2)
+    full = c == PLANE - 1
+    with phase("w_full"):
+        pl.when(full)(lambda: fetch(jnp.int32(1)))
     with phase("w_lift1"):
         lift(1)
     with phase("w_fetch1"):
-        fetch(jnp.int32(1))
+        fetch(jnp.where(full, 2, 1))
 
     @pl.when(odd == 0)
     def _():
@@ -823,7 +826,7 @@
 
         def onward():
             with phase("w_fetch"):
-                fetch(jnp.int32(2))
+                pl.when(jnp.logical_not(full))(lambda: fetch(jnp.int32(2)))
                 fetch(jnp.int32(3))
 
         with phase("single"):
@@ -856,7 +859,7 @@
 
     @pl.loop(0, pairs)
     def _(p):
-        @pl.when(p == cy)
+        @pl.when(p == 0)
         def _():
             with phase("w_lift2"):
                 lift(2)

time: 50.7 us -> 50.4 us (level)
  no operation moved by 1% of the time
where the time goes in v6:
time: 50.4 us; the launch traced here: 50 us
  Pallas kernels  49.1 us (97%)
  local copies, waits for them, and re-layouts  0.88 us (2%)
    pallas_call x1, Pallas kernels, fast_shards(): pl.pallas_call(lambda *refs: layer_kernel(count, *refs), out_shape=pltpu....  49.1 us

profile of v6, /device:TPU:27, one launch (start us, length us, event | category | flops | bytes accessed | tf_op | source)
XLA Modules:
  0.0 50.0 jit_solution(10554891981451376077)
XLA Ops:
  0.0 49.1 %layer.1 = bf16[384,1024]{1,0:T(8,128)(2,1)S(1)} custom-call(bf16[192,2048]{1,0:T(8,128)(2,1)} %refs_0_.1, f32[1,2048]{1,0:T(1,128)} %bitcast.4, bf16[128,256]{1,0:T(8,128)(2,1)} %refs_2_.1, bf16[64,128]{1,0:T(8,128)(2,1)} %bitcast.3, f32[1,256]{1,0:T(1,128)} %bitcast.5, f32[384,64]{1,0:T(8,128)} %constant.4.clone.refs_5_, ...), custom_call_target="tpu_custom_call" | custom-call | tf_op jit(solution)/shard_map/layer/pallas_call | solution.py:949
  49.1 0.9 %copy.18 = bf16[384,1024]{1,0:T(8,128)(2,1)} copy(bf16[384,1024]{1,0:T(8,128)(2,1)S(1)} %layer.1) | data formatting | bytes 1572864
